TPU v7x, 256 devices: a whole 4x4x8 slice. The times are simulated.
256 devices in a mesh: st: 64 (over z, y, core), tp: 4 (over x).
Axes of the slice: x: 4, y: 4, z: 8, core: 2. Of those that a mesh axis runs over, the one named last changes fastest.
Arguments:
- queries: bfloat16 [65536, 1024], P('st', 'tp'), may hold values from -540 to 540
- gate_pre: bfloat16 [65536, 1024], P('st', 'tp'), may hold values from -6 to 6
- cotangent: bfloat16 [65536, 1024], P('st', 'tp'), may hold values from -6 to 6
- store: bfloat16 [81920, 2048], P('st'), may hold values from -6 to 6
- store_gain: float32 [2048], replicated, may hold values from 0.1 to 1.9
- w_key: bfloat16 [2048, 1024], P(None, 'tp'), may hold values from -0.125 to 0.125
- w_value: bfloat16 [2048, 1024], P(None, 'tp'), may hold values from -0.125 to 0.125
- owners: int32 [512, 4], P('st'), may hold values from 0 to 63, all different within a row; in each aligned block of 8 rows (0 to 7, 8 to 15, ...) at most 1 rows name the same one
- slots: int32 [512, 4], P('st'), may hold values from 0 to 19
Outputs:
- grad_queries: float32 [65536, 1024], P('st', 'tp')
- grad_store: float32 [81920, 2048], P(('st', 'tp'))
- grad_w_value: float32 [2048, 1024], P('st', 'tp')
Inputs may be any that keep to these rules, and one draw needn't show every extreme that they name: Each block names 4 different owners. Among the blocks of one device no owner is named twice.
All inputs are finite; a program needn't handle non-finite values.
Results may differ from a plain program's by a relative error of at most 0.014.
Values may be sent and summed in bfloat16 or wider, within the bound.
No kernel may reach another device: no remote copies, remote signals or barrier semaphores. Data moves between devices by JAX's collectives and lax.ppermute only.
A program may use at most 192 MiB of HBM per device.

v0:
```python
import jax
import jax.numpy as jnp
from jax import lax
from jax.experimental import pallas as pl
from jax.experimental.pallas import tpu as pltpu
from jax.sharding import Mesh
from jax.sharding import PartitionSpec as P


HD = 128
PLEN = 64
EPS = 1e-06
ST = ("st_0", "st_1", "st_2")
ST_TP = ("st_0", "st_1", "st_2", "tp")
MIB = 1024 * 1024


def params(mib):
    return pltpu.CompilerParams(
        dimension_semantics=("arbitrary",), vmem_limit_bytes=mib * MIB
    )


def in_hbm(value):
    return pltpu.with_memory_space_constraint(value, pltpu.HBM)


def dot_nn(a, b):
    return lax.dot_general(a, b, (((1,), (0,)), ((), ())), preferred_element_type=jnp.float32)


def dot_nt(a, b):
    return lax.dot_general(a, b, (((1,), (1,)), ((), ())), preferred_element_type=jnp.float32)


def dot_tn(a, b):
    return lax.dot_general(a, b, (((0,), (0,)), ((), ())), preferred_element_type=jnp.float32)


def normed_rows(x, gain):
    inverse = lax.rsqrt(jnp.mean(x * x, axis=-1, keepdims=True) + EPS)
    return (x * inverse * gain).astype(jnp.bfloat16)


def tables_kernel(store_ref, gain_ref, wk_hbm, wv_hbm, table_ref, wk_ref, wv_ref, sems):
    first = pl.program_id(0) == 0
    width = wk_ref.shape[1]
    keys_in = pltpu.make_async_copy(wk_hbm, wk_ref, sems.at[0])
    values_in = pltpu.make_async_copy(wv_hbm, wv_ref, sems.at[1])

    @pl.when(first)
    def _():
        keys_in.start()
        values_in.start()

    normed = normed_rows(store_ref[...].astype(jnp.float32), gain_ref[...])

    @pl.when(first)
    def _():
        keys_in.wait()
        values_in.wait()

    table_ref[:, :width] = dot_nn(normed, wk_ref[...]).astype(jnp.bfloat16)
    table_ref[:, width:] = dot_nn(normed, wv_ref[...]).astype(jnp.bfloat16)


def key_value_tables(store, gain, w_key, w_value):
    rows, model = store.shape
    width = w_key.shape[1]
    step = 256
    return pl.pallas_call(
        tables_kernel,
        grid=(rows // step,),
        in_specs=[
            pl.BlockSpec((step, model), lambda i: (i, 0)),
            pl.BlockSpec((1, model), lambda i: (0, 0)),
            pl.BlockSpec(memory_space=pltpu.HBM),
            pl.BlockSpec(memory_space=pltpu.HBM),
        ],
        out_specs=pl.BlockSpec((step, 2 * width), lambda i: (i, 0)),
        out_shape=jax.ShapeDtypeStruct((rows, 2 * width), jnp.bfloat16),
        scratch_shapes=[
            pltpu.VMEM((model, width), jnp.bfloat16),
            pltpu.VMEM((model, width), jnp.bfloat16),
            pltpu.SemaphoreType.DMA((2,)),
        ],
        compiler_params=params(16),
        cost_estimate=pl.CostEstimate(
            flops=4 * rows * model * width, bytes_accessed=2 * rows * model, transcendentals=rows
        ),
        name="tables",
    )(in_hbm(store), in_hbm(gain), in_hbm(w_key), in_hbm(w_value))


def turned_kernel(store_ref, gain_ref, out_ref):
    normed = normed_rows(store_ref[...].astype(jnp.float32), gain_ref[...])
    out_ref[...] = normed.T


def turned_normed(store, gain):
    rows, model = store.shape
    step = 256
    return pl.pallas_call(
        turned_kernel,
        grid=(rows // step,),
        in_specs=[
            pl.BlockSpec((step, model), lambda i: (i, 0)),
            pl.BlockSpec((1, model), lambda i: (0, 0)),
        ],
        out_specs=pl.BlockSpec((model, step), lambda i: (0, i)),
        out_shape=pltpu.HBM((model, rows), jnp.bfloat16),
        compiler_params=params(16),
        cost_estimate=pl.CostEstimate(
            flops=16 * rows * model, bytes_accessed=4 * rows * model, transcendentals=rows
        ),
        name="turned_normed",
    )(in_hbm(store), in_hbm(gain))


def gather_kernel(asked_ref, table_ref, out_hbm, sems):
    copies = []
    for i in range(out_hbm.shape[0]):
        asked = jnp.maximum(asked_ref[i], 0)
        copies.append(pltpu.make_async_copy(table_ref.at[asked], out_hbm.at[i], sems.at[i]))
        copies[-1].start()
    for copy in copies:
        copy.wait()


def picked_passages(asked, table):
    _, length, width = table.shape
    slots = asked.shape[0]
    return pl.pallas_call(
        gather_kernel,
        in_specs=[
            pl.BlockSpec(memory_space=pltpu.SMEM),
            pl.BlockSpec(memory_space=pltpu.VMEM),
        ],
        out_specs=pl.BlockSpec(memory_space=pltpu.HBM),
        out_shape=pltpu.HBM((slots, length, width), jnp.bfloat16),
        scratch_shapes=[pltpu.SemaphoreType.DMA((slots,))],
        compiler_params=pltpu.CompilerParams(vmem_limit_bytes=8 * MIB),
        name="picked",
    )(asked, table)


def slot_copies(owner_ref, scratch, out_hbm, sems, at, parity):
    per_block = owner_ref.shape[0]
    each = scratch.shape[1] // per_block
    return [
        pltpu.make_async_copy(
            scratch.at[parity, b * per_block + j],
            out_hbm.at[owner_ref[j, at * each + b]],
            sems.at[parity, b * per_block + j],
        )
        for b in range(each)
        for j in range(per_block)
    ]


def wait_slots(owner_ref, scratch, out_hbm, sems):
    step = pl.program_id(0)

    @pl.when(step >= 2)
    def _():
        for copy in slot_copies(owner_ref, scratch, out_hbm, sems, step - 2, lax.rem(step, 2)):
            copy.wait()


def send_slots(owner_ref, scratch, out_hbm, sems):
    step, steps = pl.program_id(0), pl.num_programs(0)
    slot = lax.rem(step, 2)
    for copy in slot_copies(owner_ref, scratch, out_hbm, sems, step, slot):
        copy.start()

    @pl.when(step == steps - 1)
    def _():
        for copy in slot_copies(owner_ref, scratch, out_hbm, sems, step - 1, 1 - slot):
            copy.wait()
        for copy in slot_copies(owner_ref, scratch, out_hbm, sems, step, slot):
            copy.wait()


def block_units(owner_ref, q_ref, g_ref, c_ref, pieces):
    width = q_ref.shape[1]
    per_block = owner_ref.shape[0]
    each = len(pieces) // per_block
    length = q_ref.shape[0] // each
    gate = jax.nn.sigmoid(g_ref[...].astype(jnp.float32))
    grad_in = (gate * c_ref[...].astype(jnp.float32)).astype(jnp.bfloat16)
    units = []
    for b in range(each):
        for h in range(width // HD):
            rows = slice(b * length, (b + 1) * length)
            cols = slice(h * HD, (h + 1) * HD)
            own = pieces[b * per_block : (b + 1) * per_block]
            keys = jnp.concatenate([p[0, :, cols] for p in own], axis=0)
            units.append((b, rows, cols, own, q_ref[rows, cols], grad_in[rows, cols], keys))
    scores = [dot_nt(u[4], u[6]) * HD ** (-0.5) for u in units]
    weights = [jnp.exp(x - jnp.max(x, axis=-1, keepdims=True)) for x in scores]
    weights = [x / jnp.sum(x, axis=-1, keepdims=True) for x in weights]
    return units, weights


def value_slots_kernel(owner_ref, q_ref, g_ref, c_ref, *refs):
    pieces, (out_hbm, scratch, sems) = refs[:-3], refs[-3:]
    per_block = owner_ref.shape[0]
    slot = lax.rem(pl.program_id(0), 2)
    units, weights = block_units(owner_ref, q_ref, g_ref, c_ref, pieces)
    wait_slots(owner_ref, scratch, out_hbm, sems)
    for (b, _, cols, _, _, gin, _), weight in zip(units, weights):
        grad_values = dot_tn(weight.astype(jnp.bfloat16), gin).astype(jnp.bfloat16)
        for j in range(per_block):
            part = slice(j * PLEN, (j + 1) * PLEN)
            scratch[slot, b * per_block + j, :, cols] = grad_values[part]
    send_slots(owner_ref, scratch, out_hbm, sems)


def key_slots_kernel(owner_ref, q_ref, g_ref, c_ref, *refs):
    pieces, (gq_ref, out_hbm, scratch, sems) = refs[:-4], refs[-4:]
    per_block = owner_ref.shape[0]
    width = q_ref.shape[1]
    slot = lax.rem(pl.program_id(0), 2)
    units, weights = block_units(owner_ref, q_ref, g_ref, c_ref, pieces)
    grad_weights = []
    for _, _, cols, own, _, gin, _ in units:
        vcols = slice(width + cols.start, width + cols.stop)
        values = jnp.concatenate([p[0, :, vcols] for p in own], axis=0)
        grad_weights.append(dot_nt(gin, values))
    delta = [
        jnp.sum(w.astype(jnp.bfloat16).astype(jnp.float32) * g, axis=-1, keepdims=True)
        for w, g in zip(weights, grad_weights)
    ]
    halves = [(w * (g - d)).astype(jnp.bfloat16) for w, g, d in zip(weights, grad_weights, delta)]
    wait_slots(owner_ref, scratch, out_hbm, sems)
    for (b, rows, cols, _, q, _, keys), half in zip(units, halves):
        gq_ref[rows, cols] = dot_nn(half, keys) * HD ** (-0.5)
        grad_keys = (dot_tn(half, q) * HD ** (-0.5)).astype(jnp.bfloat16)
        for j in range(per_block):
            part = slice(j * PLEN, (j + 1) * PLEN)
            scratch[slot, b * per_block + j, :, cols] = grad_keys[part]
    send_slots(owner_ref, scratch, out_hbm, sems)


def attention(owner_turned, queries, gate_pre, cotangent, got, keys_only):
    rows, width = queries.shape
    per_block, blocks = owner_turned.shape
    slots, length, both = got.shape
    each = 2
    steps = blocks // each
    tokens = pl.BlockSpec((rows // steps, width), lambda i, o: (i, 0))
    read = width if keys_only else both

    def piece(b, j):
        return pl.BlockSpec((1, length, read), lambda i, o: (o[j, i * each + b], 0, 0))

    pieces = [piece(b, j) for b in range(each) for j in range(per_block)]
    keys = PLEN * per_block
    out = pltpu.HBM((slots, length, width), jnp.bfloat16)
    hbm = pl.BlockSpec(memory_space=pltpu.HBM)
    return pl.pallas_call(
        value_slots_kernel if keys_only else key_slots_kernel,
        grid_spec=pltpu.PrefetchScalarGridSpec(
            num_scalar_prefetch=1,
            grid=(steps,),
            in_specs=[tokens, tokens, tokens] + pieces,
            out_specs=[hbm] if keys_only else [tokens, hbm],
            scratch_shapes=[
                pltpu.VMEM((2, len(pieces), length, width), jnp.bfloat16),
                pltpu.SemaphoreType.DMA((2, len(pieces))),
            ],
        ),
        out_shape=[out] if keys_only else [jax.ShapeDtypeStruct((rows, width), jnp.float32), out],
        compiler_params=params(20),
        cost_estimate=pl.CostEstimate(
            flops=(4 if keys_only else 8) * rows * width * keys,
            bytes_accessed=10 * rows * width + 2 * got.size,
            transcendentals=rows * width * keys // HD,
        ),
        name="value_slots" if keys_only else "key_slots",
    )(
        owner_turned,
        in_hbm(queries),
        in_hbm(gate_pre),
        in_hbm(cotangent),
        *([in_hbm(got)] * len(pieces)),
    )


def add_asked(asked_ref, back_ref, total):
    step = pl.program_id(0)
    each = back_ref.shape[0]

    @pl.when(step == 0)
    def _():
        total[...] = jnp.zeros_like(total)

    for i in range(each):
        asked = asked_ref[step * each + i]

        @pl.when(asked >= 0)
        def _():
            total[asked] += back_ref[i].astype(jnp.float32)


def write_quarters(place_ref, total, parts):
    passages, length, _ = total.shape
    share = passages // 4
    for turn, out in enumerate(parts):
        first = lax.rem(place_ref[0] + turn, 4) * share
        for p in range(share):
            out[p * length : (p + 1) * length, :] = total[first + p].astype(jnp.bfloat16)


def value_kernel(asked_ref, place_ref, back_ref, turned_hbm, *refs):
    parts, (mine_ref, other_ref, total, terms, turned_ref, sem) = refs[:4], refs[4:]
    turned_in = pltpu.make_async_copy(turned_hbm, turned_ref, sem)

    @pl.when(pl.program_id(0) == 0)
    def _():
        turned_in.start()

    add_asked(asked_ref, back_ref, total)

    @pl.when(pl.program_id(0) == pl.num_programs(0) - 1)
    def _():
        write_quarters(place_ref, total, parts)
        passages, length, width = total.shape
        values = total[...].astype(jnp.bfloat16).reshape(passages * length, width)
        pieces, piece, _ = terms.shape
        turned_in.wait()
        made = dot_nn(turned_ref[...], values).astype(jnp.bfloat16)
        for p in range(pieces):
            terms[p] = made[p * piece : (p + 1) * piece]
        for p in range(pieces // 2):
            turn = p % 8 * 8 + p // 8 * 2
            mine_ref[p] = terms[place_ref[1] ^ turn]
            other_ref[p] = terms[place_ref[1] ^ (turn + 1)]


def value_sums(asked, place, back, turned, passages, devices):
    slots, length, width = back.shape
    model, rows = turned.shape
    each = 16
    quarter = jax.ShapeDtypeStruct((rows // 4, width), jnp.bfloat16)
    half = jax.ShapeDtypeStruct((devices // 2, model // devices, width), jnp.bfloat16)
    return pl.pallas_call(
        value_kernel,
        grid_spec=pltpu.PrefetchScalarGridSpec(
            num_scalar_prefetch=2,
            grid=(slots // each,),
            in_specs=[
                pl.BlockSpec((each, length, width), lambda i, a, t: (i, 0, 0)),
                pl.BlockSpec(memory_space=pltpu.HBM),
            ],
            out_specs=[pl.BlockSpec(quarter.shape, lambda i, a, t: (0, 0))] * 4
            + [pl.BlockSpec(half.shape, lambda i, a, t: (0, 0, 0))] * 2,
            scratch_shapes=[
                pltpu.VMEM((passages, length, width), jnp.float32),
                pltpu.VMEM((devices, model // devices, width), jnp.bfloat16),
                pltpu.VMEM((model, rows), jnp.bfloat16),
                pltpu.SemaphoreType.DMA,
            ],
        ),
        out_shape=[quarter] * 4 + [half] * 2,
        compiler_params=params(24),
        cost_estimate=pl.CostEstimate(
            flops=2 * model * rows * width, bytes_accessed=2 * model * rows, transcendentals=0
        ),
        name="value_sums",
    )(asked, place, back, in_hbm(turned))


def key_kernel(asked_ref, place_ref, back_ref, *refs):
    parts, total = refs[:4], refs[4]
    add_asked(asked_ref, back_ref, total)

    @pl.when(pl.program_id(0) == pl.num_programs(0) - 1)
    def _():
        write_quarters(place_ref, total, parts)


def key_sums(asked, place, back, passages):
    slots, length, width = back.shape
    each = 16
    quarter = jax.ShapeDtypeStruct((passages * length // 4, width), jnp.bfloat16)
    return pl.pallas_call(
        key_kernel,
        grid_spec=pltpu.PrefetchScalarGridSpec(
            num_scalar_prefetch=2,
            grid=(slots // each,),
            in_specs=[pl.BlockSpec((each, length, width), lambda i, a, t: (i, 0, 0))],
            out_specs=[pl.BlockSpec(quarter.shape, lambda i, a, t: (0, 0))] * 4,
            scratch_shapes=[pltpu.VMEM((passages, length, width), jnp.float32)],
        ),
        out_shape=[quarter] * 4,
        compiler_params=params(12),
        cost_estimate=pl.CostEstimate(
            flops=4 * back.size, bytes_accessed=2 * back.size, transcendentals=0
        ),
        name="key_sums",
    )(asked, place, back)


def near_kernel(*refs):
    count = 4
    parts, weights, out_ref = refs[:count], refs[count : 2 * count], refs[2 * count]
    held, sems = refs[2 * count + 1 : -1], refs[-1]
    width = parts[0].shape[1]
    arrivals = [
        pltpu.make_async_copy(w.at[:, width:], h, sems.at[i])
        for i, (w, h) in enumerate(zip(weights, held))
    ]
    for copy in arrivals:
        copy.start()
    made = []
    for part, arrival, h in zip(parts, arrivals, held):
        arrival.wait()
        made.append(dot_nt(part[...], h[...]))
    out_ref[...] = sum(made)


def near_products(parts, weights):
    quarter, width = parts[0].shape
    model = weights[0].shape[0]
    count = len(parts)
    vmem = pl.BlockSpec(memory_space=pltpu.VMEM)
    hbm = pl.BlockSpec(memory_space=pltpu.HBM)
    return pl.pallas_call(
        near_kernel,
        in_specs=[vmem] * count + [hbm] * count,
        out_specs=vmem,
        out_shape=jax.ShapeDtypeStruct((quarter, model), jnp.float32),
        scratch_shapes=[pltpu.VMEM((model, width), jnp.bfloat16)] * count
        + [pltpu.SemaphoreType.DMA((count,))],
        compiler_params=pltpu.CompilerParams(vmem_limit_bytes=16 * MIB),
        cost_estimate=pl.CostEstimate(
            flops=2 * count * quarter * model * width,
            bytes_accessed=2 * count * model * width,
            transcendentals=0,
        ),
        name="near_products",
    )(*parts, *[in_hbm(w) for w in weights])


def own_kernel(place_ref, part_ref, near_ref, *refs):
    count = 4
    weights, store_hbm = refs[:count], refs[count]
    out_ref, rows_ref, *keys_refs = refs[count + 1 : 2 * count + 2]
    held, sems = refs[2 * count + 2], refs[-1]
    quarter, width = part_ref.shape
    first = pl.multiple_of(place_ref[0] * quarter, quarter)
    copies = [
        pltpu.make_async_copy(w.at[:, :width], k, sems.at[i])
        for i, (w, k) in enumerate(zip(weights, [held] + keys_refs))
    ]
    copies.append(
        pltpu.make_async_copy(store_hbm.at[pl.ds(first, quarter)], rows_ref, sems.at[count])
    )
    for copy in copies:
        copy.start()
    copies[0].wait()
    out_ref[...] = near_ref[...] + dot_nt(part_ref[...], held[...])
    for copy in copies[1:]:
        copy.wait()


def own_product(place, part, near, weights, store):
    quarter, width = part.shape
    model = weights[0].shape[0]
    count = len(weights)
    vmem = pl.BlockSpec(memory_space=pltpu.VMEM)
    hbm = pl.BlockSpec(memory_space=pltpu.HBM)
    return pl.pallas_call(
        own_kernel,
        in_specs=[pl.BlockSpec(memory_space=pltpu.SMEM), vmem, vmem] + [hbm] * (count + 1),
        out_specs=[vmem] * (count + 1),
        out_shape=[
            pltpu.VMEM((quarter, model), jnp.float32),
            pltpu.VMEM((quarter, model), jnp.bfloat16),
        ]
        + [pltpu.VMEM((model, width), jnp.bfloat16)] * (count - 1),
        scratch_shapes=[
            pltpu.VMEM((model, width), jnp.bfloat16),
            pltpu.SemaphoreType.DMA((count + 1,)),
        ],
        compiler_params=pltpu.CompilerParams(vmem_limit_bytes=16 * MIB),
        cost_estimate=pl.CostEstimate(
            flops=2 * quarter * model * width,
            bytes_accessed=4 * count * model * width,
            transcendentals=0,
        ),
        name="own_product",
    )(place, part, near, *[in_hbm(w) for w in weights], in_hbm(store))


def final_kernel(rows_ref, gain_ref, near_ref, *refs):
    parts, weights, (out_hbm, out_ref, sems) = refs[:3], refs[3:6], refs[6:]
    made = near_ref[...]
    for part, weight in zip(parts, weights):
        made += dot_nt(part[...], weight[...])
    step = 64
    sent = []
    for i in range(out_ref.shape[0] // step):
        at = slice(i * step, (i + 1) * step)
        rows = rows_ref[at].astype(jnp.float32)
        inverse = lax.rsqrt(jnp.mean(rows * rows, axis=-1, keepdims=True) + EPS)
        unit = rows * inverse
        grad_unit = made[at] * gain_ref[...]
        mean = jnp.mean(grad_unit * unit, axis=-1, keepdims=True)
        out_ref[at] = inverse * (grad_unit - unit * mean)
        sent.append(pltpu.make_async_copy(out_ref.at[at], out_hbm.at[at], sems.at[i]))
        sent[-1].start()
    for copy in sent:
        copy.wait()


def store_gradient(rows, gain, near, parts, weights):
    quarter, model = rows.shape
    width = parts[0].shape[1]
    vmem = pl.BlockSpec(memory_space=pltpu.VMEM)
    return pl.pallas_call(
        final_kernel,
        in_specs=[vmem] * (3 + 2 * len(parts)),
        out_specs=pl.BlockSpec(memory_space=pltpu.HBM),
        out_shape=jax.ShapeDtypeStruct((quarter, model), jnp.float32),
        scratch_shapes=[
            pltpu.VMEM((quarter, model), jnp.float32),
            pltpu.SemaphoreType.DMA((quarter // 64,)),
        ],
        compiler_params=pltpu.CompilerParams(vmem_limit_bytes=16 * MIB),
        cost_estimate=pl.CostEstimate(
            flops=6 * quarter * model * width,
            bytes_accessed=4 * quarter * model,
            transcendentals=quarter,
        ),
        name="store_gradient",
    )(rows, gain, near, *parts, *weights)


def shifted(value, turn):
    return lax.ppermute(value, "tp", [(i, (i + turn) % 4) for i in range(4)])


def halved(value, axis, distance, kind):
    size = lax.axis_size(axis)
    half = value.shape[0] // 2
    pairs = [(i, i ^ distance) for i in range(size)]
    came = lax.ppermute(value[half:].astype(kind), axis, pairs)
    return value[:half] + came.astype(jnp.float32)


def local(queries, gate_pre, cotangent, store, store_gain, w_key, w_value, owners, slots):
    st_size = lax.axis_size(ST)
    width = queries.shape[1]
    rows_dev, model = store.shape
    passages = rows_dev // PLEN
    place = jnp.stack([lax.axis_index("tp"), lax.axis_index(ST)]).astype(jnp.int32)
    gain = store_gain.reshape(1, model)

    owner_turned = owners.T
    hits = owner_turned[None] == jnp.arange(st_size, dtype=jnp.int32)[:, None, None]
    requests = jnp.where(hits, slots.T[None], -1)
    asked = lax.all_to_all(requests, ST, split_axis=0, concat_axis=0, tiled=True)
    asked = jnp.max(asked, axis=(1, 2))

    table = key_value_tables(store, gain, w_key, w_value)
    picked = picked_passages(asked, table.reshape(passages, PLEN, 2 * width))
    got = lax.all_to_all(picked, ST, split_axis=0, concat_axis=0, tiled=True)

    late_key, late_value, _ = lax.optimization_barrier((w_key, w_value, picked))
    both = jnp.concatenate([late_key, late_value], axis=1)
    weights = [both] + [shifted(both, turn) for turn in (1, 3, 2)]
    got, *came = lax.optimization_barrier((got, *weights[1:]))
    weights = [both] + came

    (outgoing,) = attention(owner_turned, queries, gate_pre, cotangent, got, True)
    back_values = lax.all_to_all(outgoing, ST, split_axis=0, concat_axis=0, tiled=True)
    late_store, late_got, _ = lax.optimization_barrier((store, got, outgoing))
    grad_queries, outgoing = attention(
        owner_turned, queries, gate_pre, cotangent, late_got, False
    )
    turned = turned_normed(late_store, gain)
    outgoing, turned = lax.optimization_barrier((outgoing, turned))
    back_keys = lax.all_to_all(outgoing, ST, split_axis=0, concat_axis=0, tiled=True)
    back_values, turned, _ = lax.optimization_barrier((back_values, turned, grad_queries))

    own, first, second, third, mine, other = value_sums(
        asked, place, back_values, turned, passages, st_size
    )
    parts = [own, shifted(first, 1), shifted(third, 3), shifted(second, 2)]
    near = near_products(parts, weights)
    came = lax.ppermute(other, "st_2", [(0, 1), (1, 0)])
    terms = mine.astype(jnp.float32) + came.astype(jnp.float32)
    terms = halved(terms, "st_1", 2, jnp.bfloat16)
    terms = halved(terms, "st_1", 1, jnp.bfloat16)
    back_keys, near = lax.optimization_barrier((back_keys, near))
    terms = halved(terms, "st_0", 4, jnp.float32)

    own, first, second, third = key_sums(asked, place, back_keys, passages)
    own, first, second, third, terms = lax.optimization_barrier(
        (own, first, second, third, terms)
    )
    parts = []
    for part, turn in ((first, 1), (third, 3), (second, 2)):
        parts.append(shifted(part, turn))
    near, own_rows, *key_weights = own_product(place, own, near, weights, store)
    terms = halved(terms, "st_0", 2, jnp.float32)
    terms = halved(terms, "st_0", 1, jnp.float32)
    grad_w_value = terms.reshape(terms.shape[1:])
    grad_store = store_gradient(own_rows, gain, near, parts, key_weights)
    return (grad_queries, grad_store, grad_w_value)


def solution(mesh):
    torus = Mesh(mesh.devices.reshape(8, 4, 2, mesh.shape["tp"]), ("st_0", "st_1", "st_2", "tp"))
    return jax.shard_map(
        local,
        mesh=torus,
        in_specs=(
            P(ST, "tp"),
            P(ST, "tp"),
            P(ST, "tp"),
            P(ST, None),
            P(),
            P(None, "tp"),
            P(None, "tp"),
            P(ST, None),
            P(ST, None),
        ),
        out_specs=(P(ST, "tp"), P(ST_TP, None), P(ST, "tp")),
        check_vma=False,
    )
```

profile of v0, /device:TPU:2, one launch (start us, length us, event | category | flops | bytes accessed | tf_op | source)
XLA Modules:
  0.0 283.9 jit_solution(13905885159061494348)
XLA Ops:
  2.0 12.1 %all-to-all-start = ((s32[64,4,8]{2,1,0:T(4,128)}), s32[64,4,8]{2,1,0:T(4,128)S(1)}, u32[]{:S(2)}, u32[]{:S(2)}) async-start(s32[64,4,8]{2,1,0:T(4,128)} %fusion), calls=%async_computation | async-start | bytes 262144 | tf_op jit(solution)/shard_map/all_to_all | solution.py:564
  14.1 8.3 %tables.1 = bf16[1280,512]{1,0:T(8,128)(2,1)S(1)} custom-call(bf16[1280,2048]{1,0:T(8,128)(2,1)} %refs_4_.1, f32[1,2048]{1,0:T(1,128)} %bitcast.9, bf16[2048,256]{1,0:T(8,128)(2,1)} %wk_hbm.1, bf16[2048,256]{1,0:T(8,128)(2,1)} %wv_hbm.1), custom_call_target="tpu_custom_call" | custom-call | flops 2684354560 | bytes 5242880 | tf_op jit(solution)/shard_map/tables/pallas_call | solution.py:71
  22.4 2.7 all-to-all-done
  26.4 3.1 %picked.1 = bf16[64,64,512]{2,1,0:T(8,128)(2,1)} custom-call(s32[64]{0:T(128)S(1)} %reduce_max.9.asked_ref, bf16[20,64,512]{2,1,0:T(8,128)(2,1)S(1)} %bitcast.8), custom_call_target="tpu_custom_call" | custom-call | tf_op jit(solution)/shard_map/picked/pallas_call | solution.py:133
  29.5 8.0 %all-to-all-start.1 = ((bf16[64,64,512]{2,1,0:T(8,128)(2,1)}), bf16[64,64,512]{2,1,0:T(8,128)(2,1)}, u32[]{:S(2)}, u32[]{:S(2)}) async-start(bf16[64,64,512]{2,1,0:T(8,128)(2,1)} %picked.1), calls=%async_computation.1 | async-start | bytes 8388608 | tf_op jit(solution)/shard_map/all_to_all | solution.py:569
  43.1 45.9 %collective-permute-done.2.refs_7_.refs_3_ = bf16[2048,512]{1,0:T(8,128)(2,1)S(1)} collective-permute-done((bf16[2048,512]{1,0:T(8,128)(2,1)S(1)}, bf16[2048,512]{1,0:T(8,128)(2,1)S(1)}, u32[]{:S(2)}, u32[]{:S(2)}) %collective-permute-start.2) | collective-permute-done | bytes 2097184 | tf_op jit(solution)/shard_map/ppermute | solution.py:542
  89.0 43.9 %collective-permute-done.1.refs_6_.refs_2_ = bf16[2048,512]{1,0:T(8,128)(2,1)S(1)} collective-permute-done((bf16[2048,512]{1,0:T(8,128)(2,1)S(1)}, bf16[2048,512]{1,0:T(8,128)(2,1)S(1)}, u32[]{:S(2)}, u32[]{:S(2)}) %collective-permute-start.1) | collective-permute-done | bytes 2097184 | tf_op jit(solution)/shard_map/ppermute | solution.py:542
  134.2 6.1 %value_slots.1 = bf16[64,64,256]{2,1,0:T(8,128)(2,1)} custom-call(s32[4,8]{1,0:T(4,128)S(1)} %bitcast.13, bf16[1024,256]{1,0:T(8,128)(2,1)} %q_ref.3, bf16[1024,256]{1,0:T(8,128)(2,1)} %g_ref.3, bf16[1024,256]{1,0:T(8,128)(2,1)} %c_ref.3, bf16[64,64,512]{2,1,0:T(8,128)(2,1)} %all-to-all-done.1.refs_0_.refs_1_.refs_2_.refs_3_.refs_4_.refs_5_.refs_6_.refs_7_, ...), custom_call_target="tpu_custom_call" | custom-call | flops 268435456 | bytes 6815744 | tf_op jit(solution)/shard_map/value_slots/pallas_call | solution.py:261
  140.3 10.4 %all-to-all-start.3 = ((bf16[64,64,256]{2,1,0:T(8,128)(2,1)}), bf16[64,64,256]{2,1,0:T(8,128)(2,1)S(1)}, u32[]{:S(2)}, u32[]{:S(2)}) async-start(bf16[64,64,256]{2,1,0:T(8,128)(2,1)} %value_slots.1), calls=%async_computation.3 | async-start | bytes 4194304 | tf_op jit(solution)/shard_map/all_to_all | solution.py:578
  150.7 7.8 %turned_normed.1.turned_hbm = bf16[2048,1280]{1,0:T(8,128)(2,1)} custom-call(bf16[1280,2048]{1,0:T(8,128)(2,1)} %refs_4_.1, f32[1,2048]{1,0:T(1,128)} %bitcast.10), custom_call_target="tpu_custom_call" | custom-call | flops 41943040 | bytes 10485760 | tf_op jit(solution)/shard_map/turned_normed/pallas_call | solution.py:103
  158.4 7.5 %key_slots.1 = (f32[1024,256]{1,0:T(8,128)}, bf16[64,64,256]{2,1,0:T(8,128)(2,1)}) custom-call(s32[4,8]{1,0:T(4,128)S(1)} %bitcast.14, bf16[1024,256]{1,0:T(8,128)(2,1)} %q_ref.3, bf16[1024,256]{1,0:T(8,128)(2,1)} %g_ref.3, bf16[1024,256]{1,0:T(8,128)(2,1)} %c_ref.3, ...), custom_call_target="tpu_custom_call" | custom-call | flops 536870912 | bytes 6815744 | tf_op jit(solution)/shard_map/key_slots/pallas_call | solution.py:261
  165.9 36.1 %all-to-all-done.3.back_ref = bf16[64,64,256]{2,1,0:T(8,128)(2,1)S(1)} async-done(((bf16[64,64,256]{2,1,0:T(8,128)(2,1)}), bf16[64,64,256]{2,1,0:T(8,128)(2,1)S(1)}, u32[]{:S(2)}, u32[]{:S(2)}) %all-to-all-start.3) | async-done | bytes 2097184 | tf_op jit(solution)/shard_map/all_to_all | solution.py:578
  202.0 5.8 %all-to-all-start.2 = ((bf16[64,64,256]{2,1,0:T(8,128)(2,1)}), bf16[64,64,256]{2,1,0:T(8,128)(2,1)}, u32[]{:S(2)}, u32[]{:S(2)}) async-start(bf16[64,64,256]{2,1,0:T(8,128)(2,1)} %get-tuple-element.46), calls=%async_computation.2 | async-start | bytes 4194304 | tf_op jit(solution)/shard_map/all_to_all | solution.py:585
  207.9 4.7 %value_sums.1 = (bf16[320,256]{1,0:T(8,128)(2,1)S(1)}, bf16[320,256]{1,0:T(8,128)(2,1)S(1)}, bf16[320,256]{1,0:T(8,128)(2,1)S(1)}, bf16[320,256]{1,0:T(8,128)(2,...) custom-call(s32[64]{0:T(128)S(1)} %reduce_max.9.asked_ref, s32[2]{0:T(128)S(1)} %pad_add_fusion.place_ref, ...), custom_call_target="tpu_custom_call" | custom-call | flops 1342177280 | bytes 5242880 | tf_op jit(solution)/shard_map/value_sums/pallas_call | solution.py:347
  214.8 2.9 %collective-permute-start.7 = (bf16[16,32,256]{2,1,0:T(8,128)(2,1)S(1)}, bf16[16,32,256]{2,1,0:T(8,128)(2,1)S(1)}, u32[]{:S(2)}, u32[]{:S(2)}) collective-permute-start(bf16[16,32,256]{2,1,0:T(8,128)(2,1)S(1)} %slice.59), channel_id=1, source_target_pairs={{0,16},{8,24},{16,0},{24,8},{1,17},{9,25},{17,1},{25,9},{2,18},{10... | collective-permute-start | bytes 786440 | tf_op jit(solution)/shard_map/ppermute | solution.py:549
  217.7 12.8 %collective-permute-done.7 = bf16[16,32,256]{2,1,0:T(8,128)(2,1)S(1)} collective-permute-done((bf16[16,32,256]{2,1,0:T(8,128)(2,1)S(1)}, bf16[16,32,256]{2,1,0:T(8,128)(2,1)S(1)}, u32[]{:S(2)}, u32[]{:S(2)}) %collective-permute-start.7) | collective-permute-done | bytes 262176 | tf_op jit(solution)/shard_map/ppermute | solution.py:549
  235.0 3.3 %collective-permute-done.8 = bf16[8,32,256]{2,1,0:T(8,128)(2,1)S(1)} collective-permute-done((bf16[8,32,256]{2,1,0:T(8,128)(2,1)S(1)}, bf16[8,32,256]{2,1,0:T(8,128)(2,1)S(1)}, u32[]{:S(2)}, u32[]{:S(2)}) %collective-permute-start.8) | collective-permute-done | bytes 131104 | tf_op jit(solution)/shard_map/ppermute | solution.py:549
  238.3 4.8 %collective-permute-start.9 = (f32[4,32,256]{2,1,0:T(8,128)S(1)}, f32[4,32,256]{2,1,0:T(8,128)S(1)}, u32[]{:S(2)}, u32[]{:S(2)}) collective-permute-start(f32[4,32,256]{2,1,0:T(8,128)S(1)} %slice.47), channel_id=1, source_target_pairs={{0,128},{32,160},{64,192},{96,224},{128,0},{160,32},{192,64},{224,... | collective-permute-start | bytes 393224 | tf_op jit(solution)/shard_map/ppermute | solution.py:549
  243.1 3.4 %near_products.1.near_ref = f32[320,2048]{1,0:T(8,128)S(1)} custom-call(bf16[320,256]{1,0:T(8,128)(2,1)S(1)} %get-tuple-element.50.refs_0_, bf16[320,256]{1,0:T(8,128)(2,1)S(1)} %collective-permute-done.3.refs_1_, bf16[320,256]{1,0:T(8,128)(2,1)S(1)} %collective-permute-done.4.refs_2_, bf16[320,256]{1,0:T(8,128)(2,1)S(1)} %collective-permute-done.5.refs_3_, ...), custom_call_target="tpu_custom_call" | custom-call | flops 1342177280 | bytes 4194304 | tf_op jit(solution)/shard_map/near_products/pallas_call | solution.py:429
  246.5 12.0 %all-to-all-done.2.back_ref = bf16[64,64,256]{2,1,0:T(8,128)(2,1)} async-done(((bf16[64,64,256]{2,1,0:T(8,128)(2,1)}), bf16[64,64,256]{2,1,0:T(8,128)(2,1)}, u32[]{:S(2)}, u32[]{:S(2)}) %all-to-all-start.2) | async-done | bytes 2097184 | tf_op jit(solution)/shard_map/all_to_all | solution.py:585
  258.5 3.4 %key_sums.1 = (bf16[320,256]{1,0:T(8,128)(2,1)S(1)}, bf16[320,256]{1,0:T(8,128)(2,1)S(1)}, bf16[320,256]{1,0:T(8,128)(2,1)S(1)}, bf16[320,256]{1,0:T(8,128)(2,1)S(1)}) custom-call(s32[64]{0:T(128)S(1)} %reduce_max.9.asked_ref, s32[2]{0:T(128)S(1)} %pad_add_fusion.place_ref, bf16[64,64,256]{2,1,0:T(8,128)(2,1)} %all-to-all-done.2.back_ref), custom_call_target="tpu_custom_call" | custom-call | flops 4194304 | bytes 2097152 | tf_op jit(solution)/shard_map/key_sums/pallas_call | solution.py:387
  265.1 5.3 %collective-permute-done.13 = f32[2,32,256]{2,1,0:T(8,128)S(1)} collective-permute-done((f32[2,32,256]{2,1,0:T(8,128)S(1)}, f32[2,32,256]{2,1,0:T(8,128)S(1)}, u32[]{:S(2)}, u32[]{:S(2)}) %collective-permute-start.13) | collective-permute-done | bytes 65568 | tf_op jit(solution)/shard_map/ppermute | solution.py:549
  274.7 3.2 %own_product.1 = (f32[320,2048]{1,0:T(8,128)S(1)}, bf16[320,2048]{1,0:T(8,128)(2,1)S(1)}, bf16[2048,256]{1,0:T(8,128)(2,1)S(1)}, bf16[2048,256]{1,0:T(8,128)(2,1)S(1)}, bf16[2048,256]{1,0:T(8,128)(2,1)S(1)}) custom-call(s32[2]{0:T(128)S(1)} %pad_add_fusion.place_ref, bf16[320,256]{1,0:T(8,128)(2,1)S(1)} %get-tuple-element.64.part_ref, ...), custom_call_target="tpu_custom_call" | custom-call | flops 335544320 | bytes 8388608 | tf_op jit(solution)/shard_map/own_product/pallas_call | solution.py:474
  280.4 3.4 %store_gradient.1 = f32[320,2048]{1,0:T(8,128)} custom-call(bf16[320,2048]{1,0:T(8,128)(2,1)S(1)} %get-tuple-element.66.rows_ref, f32[1,2048]{1,0:T(1,128)S(1)} %bitcast.11, f32[320,2048]{1,0:T(8,128)S(1)} %get-tuple-element.67.near_ref, bf16[320,256]{1,0:T(8,128)(2,1)S(1)} %collective-permute-done.10.refs_0_, ...), custom_call_target="tpu_custom_call" | custom-call | flops 1006632960 | bytes 2621440 | tf_op jit(solution)/shard_map/store_gradient/pallas_call | solution.py:522
  (54 shorter events, 26.2 us)
Async XLA Ops:
  2.0 23.1 %all-to-all-start = ((s32[64,4,8]{2,1,0:T(4,128)}), s32[64,4,8]{2,1,0:T(4,128)S(1)}, u32[]{:S(2)}, u32[]{:S(2)}) async-start(s32[64,4,8]{2,1,0:T(4,128)} %fusion), calls=%async_computation | async-start | bytes 262144 | tf_op jit(solution)/shard_map/all_to_all | solution.py:564
  29.5 8.0 %copy-start.5 = (bf16[2048,256]{1,0:T(8,128)(2,1)S(1)}, bf16[2048,256]{1,0:T(8,128)(2,1)}, u32[]{:S(2)}) copy-start(bf16[2048,256]{1,0:T(8,128)(2,1)} %wk_hbm.1) | copy-start | bytes 3145732
  29.5 104.7 %all-to-all-start.1 = ((bf16[64,64,512]{2,1,0:T(8,128)(2,1)}), bf16[64,64,512]{2,1,0:T(8,128)(2,1)}, u32[]{:S(2)}, u32[]{:S(2)}) async-start(bf16[64,64,512]{2,1,0:T(8,128)(2,1)} %picked.1), calls=%async_computation.1 | async-start | bytes 8388608 | tf_op jit(solution)/shard_map/all_to_all | solution.py:569
  37.5 96.7 %copy-start.1 = (s32[8,4]{0,1:T(4,128)S(1)}, s32[8,4]{0,1:T(4,128)}, u32[]{:S(2)}) copy-start(s32[8,4]{0,1:T(4,128)} %param.16) | copy-start | bytes 388
  38.8 3.7 %copy-start.2 = (bf16[2048,512]{1,0:T(8,128)(2,1)}, bf16[2048,512]{1,0:T(8,128)(2,1)S(1)}, u32[]{:S(2)}) copy-start(bf16[2048,512]{1,0:T(8,128)(2,1)S(1)} %constant_dynamic-update-slice_fusion.refs_4_.refs_0_) | copy-start | bytes 6291460
  38.8 50.1 %collective-permute-start.2 = (bf16[2048,512]{1,0:T(8,128)(2,1)S(1)}, bf16[2048,512]{1,0:T(8,128)(2,1)S(1)}, u32[]{:S(2)}, u32[]{:S(2)}) collective-permute-start(bf16[2048,512]{1,0:T(8,128)(2,1)S(1)} %constant_dynamic-update-slice_fusion.refs_4_.refs_0_), channel_id=1, source_target_pairs={{0,2},{1,3},{2,0},{3,1},{4,6},{5,7},{6,4},{7,5},{8,10},{9,11},{10,... | collective-permute-start | bytes 6291464 | tf_op jit(solution)/shard_map/ppermute | solution.py:542
  41.0 91.8 %collective-permute-start.1 = (bf16[2048,512]{1,0:T(8,128)(2,1)S(1)}, bf16[2048,512]{1,0:T(8,128)(2,1)S(1)}, u32[]{:S(2)}, u32[]{:S(2)}) collective-permute-start(bf16[2048,512]{1,0:T(8,128)(2,1)S(1)} %constant_dynamic-update-slice_fusion.refs_4_.refs_0_), channel_id=1, source_target_pairs={{0,3},{1,0},{2,1},{3,2},{4,7},{5,4},{6,5},{7,6},{8,11},{9,8},{10,9... | collective-permute-start | bytes 6291464 | tf_op jit(solution)/shard_map/ppermute | solution.py:542
  42.5 91.7 %collective-permute-start = (bf16[2048,512]{1,0:T(8,128)(2,1)S(1)}, bf16[2048,512]{1,0:T(8,128)(2,1)}, u32[]{:S(2)}, u32[]{:S(2)}) collective-permute-start(bf16[2048,512]{1,0:T(8,128)(2,1)S(1)} %constant_dynamic-update-slice_fusion.refs_4_.refs_0_), channel_id=1, source_target_pairs={{0,1},{1,2},{2,3},{3,0},{4,5},{5,6},{6,7},{7,4},{8,9},{9,10},{10,1... | collective-permute-start | bytes 6291464 | tf_op jit(solution)/shard_map/ppermute | solution.py:542
  89.0 43.9 %copy-start.3 = (bf16[2048,512]{1,0:T(8,128)(2,1)}, bf16[2048,512]{1,0:T(8,128)(2,1)S(1)}, u32[]{:S(2)}) copy-start(bf16[2048,512]{1,0:T(8,128)(2,1)S(1)} %collective-permute-done.2.refs_7_.refs_3_) | copy-start | bytes 6291460
  140.3 61.7 %all-to-all-start.3 = ((bf16[64,64,256]{2,1,0:T(8,128)(2,1)}), bf16[64,64,256]{2,1,0:T(8,128)(2,1)S(1)}, u32[]{:S(2)}, u32[]{:S(2)}) async-start(bf16[64,64,256]{2,1,0:T(8,128)(2,1)} %value_slots.1), calls=%async_computation.3 | async-start | bytes 4194304 | tf_op jit(solution)/shard_map/all_to_all | solution.py:578
  202.0 56.5 %all-to-all-start.2 = ((bf16[64,64,256]{2,1,0:T(8,128)(2,1)}), bf16[64,64,256]{2,1,0:T(8,128)(2,1)}, u32[]{:S(2)}, u32[]{:S(2)}) async-start(bf16[64,64,256]{2,1,0:T(8,128)(2,1)} %get-tuple-element.46), calls=%async_computation.2 | async-start | bytes 4194304 | tf_op jit(solution)/shard_map/all_to_all | solution.py:585
  212.6 2.0 collective-permute-start.6
  214.8 15.7 %collective-permute-start.7 = (bf16[16,32,256]{2,1,0:T(8,128)(2,1)S(1)}, bf16[16,32,256]{2,1,0:T(8,128)(2,1)S(1)}, u32[]{:S(2)}, u32[]{:S(2)}) collective-permute-start(bf16[16,32,256]{2,1,0:T(8,128)(2,1)S(1)} %slice.59), channel_id=1, source_target_pairs={{0,16},{8,24},{16,0},{24,8},{1,17},{9,25},{17,1},{25,9},{2,18},{10... | collective-permute-start | bytes 786440 | tf_op jit(solution)/shard_map/ppermute | solution.py:549
  230.6 7.6 %collective-permute-start.8 = (bf16[8,32,256]{2,1,0:T(8,128)(2,1)S(1)}, bf16[8,32,256]{2,1,0:T(8,128)(2,1)S(1)}, u32[]{:S(2)}, u32[]{:S(2)}) collective-permute-start(bf16[8,32,256]{2,1,0:T(8,128)(2,1)S(1)} %slice.60), channel_id=1, source_target_pairs={{0,8},{8,0},{16,24},{24,16},{1,9},{9,1},{17,25},{25,17},{2,10},{10... | collective-permute-start | bytes 393224 | tf_op jit(solution)/shard_map/ppermute | solution.py:549
  230.7 12.3 %collective-permute-start.3 = (bf16[320,256]{1,0:T(8,128)(2,1)S(1)}, bf16[320,256]{1,0:T(8,128)(2,1)S(1)}, u32[]{:S(2)}, u32[]{:S(2)}) collective-permute-start(bf16[320,256]{1,0:T(8,128)(2,1)S(1)} %get-tuple-element.51), channel_id=1, source_target_pairs={{0,1},{1,2},{2,3},{3,0},{4,5},{5,6},{6,7},{7,4},{8,9},{9,10},{10,1... | collective-permute-start | bytes 491528 | tf_op jit(solution)/shard_map/ppermute | solution.py:542
  231.4 11.7 %collective-permute-start.4 = (bf16[320,256]{1,0:T(8,128)(2,1)S(1)}, bf16[320,256]{1,0:T(8,128)(2,1)S(1)}, u32[]{:S(2)}, u32[]{:S(2)}) collective-permute-start(bf16[320,256]{1,0:T(8,128)(2,1)S(1)} %get-tuple-element.52), channel_id=1, source_target_pairs={{0,3},{1,0},{2,1},{3,2},{4,7},{5,4},{6,5},{7,6},{8,11},{9,8},{10,9... | collective-permute-start | bytes 491528 | tf_op jit(solution)/shard_map/ppermute | solution.py:542
  232.8 10.2 %collective-permute-start.5 = (bf16[320,256]{1,0:T(8,128)(2,1)S(1)}, bf16[320,256]{1,0:T(8,128)(2,1)S(1)}, u32[]{:S(2)}, u32[]{:S(2)}) collective-permute-start(bf16[320,256]{1,0:T(8,128)(2,1)S(1)} %get-tuple-element.53), channel_id=1, source_target_pairs={{0,2},{1,3},{2,0},{3,1},{4,6},{5,7},{6,4},{7,5},{8,10},{9,11},{10,... | collective-permute-start | bytes 491528 | tf_op jit(solution)/shard_map/ppermute | solution.py:542
  238.3 26.1 %collective-permute-start.9 = (f32[4,32,256]{2,1,0:T(8,128)S(1)}, f32[4,32,256]{2,1,0:T(8,128)S(1)}, u32[]{:S(2)}, u32[]{:S(2)}) collective-permute-start(f32[4,32,256]{2,1,0:T(8,128)S(1)} %slice.47), channel_id=1, source_target_pairs={{0,128},{32,160},{64,192},{96,224},{128,0},{160,32},{192,64},{224,... | collective-permute-start | bytes 393224 | tf_op jit(solution)/shard_map/ppermute | solution.py:549
  264.3 6.0 %collective-permute-start.13 = (f32[2,32,256]{2,1,0:T(8,128)S(1)}, f32[2,32,256]{2,1,0:T(8,128)S(1)}, u32[]{:S(2)}, u32[]{:S(2)}) collective-permute-start(f32[2,32,256]{2,1,0:T(8,128)S(1)} %slice.39), channel_id=1, source_target_pairs={{0,64},{32,96},{64,0},{96,32},{128,192},{160,224},{192,128},{224,1... | collective-permute-start | bytes 196616 | tf_op jit(solution)/shard_map/ppermute | solution.py:549
  270.3 10.0 %copy-start = (f32[2048]{0:T(1024)S(1)}, f32[2048]{0:T(1024)}, u32[]{:S(2)}) copy-start(f32[2048]{0:T(1024)} %param.13) | copy-start | bytes 24580
  270.4 7.5 %collective-permute-start.14 = (f32[1,32,256]{2,1,0:T(8,128)S(1)}, f32[1,32,256]{2,1,0:T(8,128)S(1)}, u32[]{:S(2)}, u32[]{:S(2)}) collective-permute-start(f32[1,32,256]{2,1,0:T(8,128)S(1)} %slice.49), channel_id=1, source_target_pairs={{0,32},{32,0},{64,96},{96,64},{128,160},{160,128},{192,224},{224,1... | collective-permute-start | bytes 98312 | tf_op jit(solution)/shard_map/ppermute | solution.py:549
  270.5 8.0 %collective-permute-start.10 = (bf16[320,256]{1,0:T(8,128)(2,1)S(1)}, bf16[320,256]{1,0:T(8,128)(2,1)S(1)}, u32[]{:S(2)}, u32[]{:S(2)}) collective-permute-start(bf16[320,256]{1,0:T(8,128)(2,1)S(1)} %get-tuple-element.68), channel_id=1, source_target_pairs={{0,1},{1,2},{2,3},{3,0},{4,5},{5,6},{6,7},{7,4},{8,9},{9,10},{10,1... | collective-permute-start | bytes 491528 | tf_op jit(solution)/shard_map/ppermute | solution.py:542
  271.1 7.4 %collective-permute-start.11 = (bf16[320,256]{1,0:T(8,128)(2,1)S(1)}, bf16[320,256]{1,0:T(8,128)(2,1)S(1)}, u32[]{:S(2)}, u32[]{:S(2)}) collective-permute-start(bf16[320,256]{1,0:T(8,128)(2,1)S(1)} %get-tuple-element.69), channel_id=1, source_target_pairs={{0,3},{1,0},{2,1},{3,2},{4,7},{5,4},{6,5},{7,6},{8,11},{9,8},{10,9... | collective-permute-start | bytes 491528 | tf_op jit(solution)/shard_map/ppermute | solution.py:542
  272.6 7.8 %collective-permute-start.12 = (bf16[320,256]{1,0:T(8,128)(2,1)S(1)}, bf16[320,256]{1,0:T(8,128)(2,1)S(1)}, u32[]{:S(2)}, u32[]{:S(2)}) collective-permute-start(bf16[320,256]{1,0:T(8,128)(2,1)S(1)} %get-tuple-element.70), channel_id=1, source_target_pairs={{0,2},{1,3},{2,0},{3,1},{4,6},{5,7},{6,4},{7,5},{8,10},{9,11},{10,... | collective-permute-start | bytes 491528 | tf_op jit(solution)/shard_map/ppermute | solution.py:542
  (2 other events, 2.6 us)
where the time goes:
time: 285 us; the launch traced here: 284 us
  waiting for transfers between devices  168 us (59%)
  starting transfers between devices  57.7 us (20%)
  Pallas kernels  50.7 us (18%)
  other arithmetic  3.6 us (1%)
    ppermute x9, waiting for transfers between devices, shifted(): return lax.ppermute(value, 'tp', [(i, (i + turn) % 4) for i in range(4)])  91.7 us
    all_to_all x2, waiting for transfers between devices, local(): lax.all_to_all(outgoing, ST, split_axis=0, concat_axis=0, tiled=True)  48.1 us
    ppermute x5, waiting for transfers between devices, halved(): came = lax.ppermute(value[half:].astype(kind), axis, pairs)  23.8 us
    all_to_all x2, starting transfers between devices, local(): lax.all_to_all(outgoing, ST, split_axis=0, concat_axis=0, tiled=True)  16.2 us
    pallas_call x2, Pallas kernels, attention(): pl.pallas_call(value_slots_kernel if keys_only else key_slots_kernel, gri...  13.5 us
    ppermute x9, starting transfers between devices, shifted(): return lax.ppermute(value, 'tp', [(i, (i + turn) % 4) for i in range(4)])  12.7 us
    all_to_all x1, starting transfers between devices, local(): lax.all_to_all(requests, ST, split_axis=0, concat_axis=0, tiled=True)  12.1 us
    ppermute x5, starting transfers between devices, halved(): came = lax.ppermute(value[half:].astype(kind), axis, pairs)  8.62 us
  transfers between devices with their start and end apart: 19, of which 11 were waited for; matrix products, arithmetic and copies ran while one was open for 0% of the time, Pallas kernels for 13%

commit v1 on v0

--- a/solution.py
+++ b/solution.py
@@ -42,9 +42,12 @@
     return (x * inverse * gain).astype(jnp.bfloat16)
 
 
-def tables_kernel(store_ref, gain_ref, wk_hbm, wv_hbm, table_ref, wk_ref, wv_ref, sems):
+def tables_kernel(store_ref, gain_ref, wk_hbm, wv_hbm, table_ref, both_hbm, wk_ref, wv_ref, sems):
     first = pl.program_id(0) == 0
+    last = pl.program_id(0) == pl.num_programs(0) - 1
     width = wk_ref.shape[1]
+    keys_out = pltpu.make_async_copy(wk_ref, both_hbm.at[:, :width], sems.at[2])
+    values_out = pltpu.make_async_copy(wv_ref, both_hbm.at[:, width:], sems.at[3])
     keys_in = pltpu.make_async_copy(wk_hbm, wk_ref, sems.at[0])
     values_in = pltpu.make_async_copy(wv_hbm, wv_ref, sems.at[1])
 
@@ -59,9 +62,16 @@
     def _():
         keys_in.wait()
         values_in.wait()
+        keys_out.start()
+        values_out.start()
 
     table_ref[:, :width] = dot_nn(normed, wk_ref[...]).astype(jnp.bfloat16)
     table_ref[:, width:] = dot_nn(normed, wv_ref[...]).astype(jnp.bfloat16)
+
+    @pl.when(last)
+    def _():
+        keys_out.wait()
+        values_out.wait()
 
 
 def key_value_tables(store, gain, w_key, w_value):
@@ -77,12 +87,18 @@
             pl.BlockSpec(memory_space=pltpu.HBM),
             pl.BlockSpec(memory_space=pltpu.HBM),
         ],
-        out_specs=pl.BlockSpec((step, 2 * width), lambda i: (i, 0)),
-        out_shape=jax.ShapeDtypeStruct((rows, 2 * width), jnp.bfloat16),
+        out_specs=[
+            pl.BlockSpec((step, 2 * width), lambda i: (i, 0)),
+            pl.BlockSpec(memory_space=pltpu.HBM),
+        ],
+        out_shape=[
+            jax.ShapeDtypeStruct((rows, 2 * width), jnp.bfloat16),
+            pltpu.HBM((model, 2 * width), jnp.bfloat16),
+        ],
         scratch_shapes=[
             pltpu.VMEM((model, width), jnp.bfloat16),
             pltpu.VMEM((model, width), jnp.bfloat16),
-            pltpu.SemaphoreType.DMA((2,)),
+            pltpu.SemaphoreType.DMA((4,)),
         ],
         compiler_params=params(16),
         cost_estimate=pl.CostEstimate(
@@ -196,9 +212,9 @@
             own = pieces[b * per_block : (b + 1) * per_block]
             keys = jnp.concatenate([p[0, :, cols] for p in own], axis=0)
             units.append((b, rows, cols, own, q_ref[rows, cols], grad_in[rows, cols], keys))
-    scores = [dot_nt(u[4], u[6]) * HD ** (-0.5) for u in units]
-    weights = [jnp.exp(x - jnp.max(x, axis=-1, keepdims=True)) for x in scores]
-    weights = [x / jnp.sum(x, axis=-1, keepdims=True) for x in weights]
+    scores = [dot_nt(u[6], u[4]) * HD ** (-0.5) for u in units]
+    weights = [jnp.exp(x - jnp.max(x, axis=0, keepdims=True)) for x in scores]
+    weights = [x * (1.0 / jnp.sum(x, axis=0, keepdims=True)) for x in weights]
     return units, weights
 
 
@@ -209,7 +225,7 @@
     units, weights = block_units(owner_ref, q_ref, g_ref, c_ref, pieces)
     wait_slots(owner_ref, scratch, out_hbm, sems)
     for (b, _, cols, _, _, gin, _), weight in zip(units, weights):
-        grad_values = dot_tn(weight.astype(jnp.bfloat16), gin).astype(jnp.bfloat16)
+        grad_values = dot_nn(weight.astype(jnp.bfloat16), gin).astype(jnp.bfloat16)
         for j in range(per_block):
             part = slice(j * PLEN, (j + 1) * PLEN)
             scratch[slot, b * per_block + j, :, cols] = grad_values[part]
@@ -226,16 +242,16 @@
     for _, _, cols, own, _, gin, _ in units:
         vcols = slice(width + cols.start, width + cols.stop)
         values = jnp.concatenate([p[0, :, vcols] for p in own], axis=0)
-        grad_weights.append(dot_nt(gin, values))
+        grad_weights.append(dot_nt(values, gin))
     delta = [
-        jnp.sum(w.astype(jnp.bfloat16).astype(jnp.float32) * g, axis=-1, keepdims=True)
+        jnp.sum(w.astype(jnp.bfloat16).astype(jnp.float32) * g, axis=0, keepdims=True)
         for w, g in zip(weights, grad_weights)
     ]
     halves = [(w * (g - d)).astype(jnp.bfloat16) for w, g, d in zip(weights, grad_weights, delta)]
     wait_slots(owner_ref, scratch, out_hbm, sems)
     for (b, rows, cols, _, q, _, keys), half in zip(units, halves):
-        gq_ref[rows, cols] = dot_nn(half, keys) * HD ** (-0.5)
-        grad_keys = (dot_tn(half, q) * HD ** (-0.5)).astype(jnp.bfloat16)
+        gq_ref[rows, cols] = dot_tn(half, keys) * HD ** (-0.5)
+        grad_keys = (dot_nn(half, q) * HD ** (-0.5)).astype(jnp.bfloat16)
         for j in range(per_block):
             part = slice(j * PLEN, (j + 1) * PLEN)
             scratch[slot, b * per_block + j, :, cols] = grad_keys[part]
@@ -373,28 +389,29 @@
 
 def key_kernel(asked_ref, place_ref, back_ref, *refs):
     parts, total = refs[:4], refs[4]
-    add_asked(asked_ref, back_ref, total)
-
-    @pl.when(pl.program_id(0) == pl.num_programs(0) - 1)
-    def _():
-        write_quarters(place_ref, total, parts)
+    total[...] = jnp.zeros_like(total)
+    for r in range(back_ref.shape[0]):
+        asked = asked_ref[r]
+
+        @pl.when(asked >= 0)
+        def _():
+            total[asked] += back_ref[r].astype(jnp.float32)
+
+    write_quarters(place_ref, total, parts)
 
 
 def key_sums(asked, place, back, passages):
-    slots, length, width = back.shape
-    each = 16
+    _, length, width = back.shape
     quarter = jax.ShapeDtypeStruct((passages * length // 4, width), jnp.bfloat16)
+    smem = pl.BlockSpec(memory_space=pltpu.SMEM)
+    vmem = pl.BlockSpec(memory_space=pltpu.VMEM)
     return pl.pallas_call(
         key_kernel,
-        grid_spec=pltpu.PrefetchScalarGridSpec(
-            num_scalar_prefetch=2,
-            grid=(slots // each,),
-            in_specs=[pl.BlockSpec((each, length, width), lambda i, a, t: (i, 0, 0))],
-            out_specs=[pl.BlockSpec(quarter.shape, lambda i, a, t: (0, 0))] * 4,
-            scratch_shapes=[pltpu.VMEM((passages, length, width), jnp.float32)],
-        ),
+        in_specs=[smem, smem, vmem],
+        out_specs=[vmem] * 4,
         out_shape=[quarter] * 4,
-        compiler_params=params(12),
+        scratch_shapes=[pltpu.VMEM((passages, length, width), jnp.float32)],
+        compiler_params=pltpu.CompilerParams(vmem_limit_bytes=12 * MIB),
         cost_estimate=pl.CostEstimate(
             flops=4 * back.size, bytes_accessed=2 * back.size, transcendentals=0
         ),
@@ -564,12 +581,11 @@
     asked = lax.all_to_all(requests, ST, split_axis=0, concat_axis=0, tiled=True)
     asked = jnp.max(asked, axis=(1, 2))
 
-    table = key_value_tables(store, gain, w_key, w_value)
+    table, both = key_value_tables(store, gain, w_key, w_value)
     picked = picked_passages(asked, table.reshape(passages, PLEN, 2 * width))
     got = lax.all_to_all(picked, ST, split_axis=0, concat_axis=0, tiled=True)
 
-    late_key, late_value, _ = lax.optimization_barrier((w_key, w_value, picked))
-    both = jnp.concatenate([late_key, late_value], axis=1)
+    both, _ = lax.optimization_barrier((both, picked))
     weights = [both] + [shifted(both, turn) for turn in (1, 3, 2)]
     got, *came = lax.optimization_barrier((got, *weights[1:]))
     weights = [both] + came

time: 285 us -> 284 us (level)
  transfers between devices with their start and end apart: 19 -> 19, of which waited for: 11 -> 12; matrix products, arithmetic and copies ran while one was open for 0% -> 0% of each run, Pallas kernels for 13% -> 13%
where the time goes in v1:
time: 284 us; the launch traced here: 283 us
  waiting for transfers between devices  170 us (60%)
  starting transfers between devices  56.9 us (20%)
  Pallas kernels  49.3 us (17%)
  other arithmetic  3.6 us (1%)
    ppermute x9, waiting for transfers between devices, shifted(): return lax.ppermute(value, 'tp', [(i, (i + turn) % 4) for i in range(4)])  91.7 us
    all_to_all x2, waiting for transfers between devices, local(): lax.all_to_all(outgoing, ST, split_axis=0, concat_axis=0, tiled=True)  48.3 us
    ppermute x5, waiting for transfers between devices, halved(): came = lax.ppermute(value[half:].astype(kind), axis, pairs)  24.8 us
    all_to_all x2, starting transfers between devices, local(): lax.all_to_all(outgoing, ST, split_axis=0, concat_axis=0, tiled=True)  15.4 us
    pallas_call x2, Pallas kernels, attention(): pl.pallas_call(value_slots_kernel if keys_only else key_slots_kernel, gri...  13.2 us
    ppermute x9, starting transfers between devices, shifted(): return lax.ppermute(value, 'tp', [(i, (i + turn) % 4) for i in range(4)])  12.7 us
    all_to_all x1, starting transfers between devices, local(): lax.all_to_all(requests, ST, split_axis=0, concat_axis=0, tiled=True)  12.1 us
    ppermute x5, starting transfers between devices, halved(): came = lax.ppermute(value[half:].astype(kind), axis, pairs)  8.62 us
  transfers between devices with their start and end apart: 19, of which 12 were waited for; matrix products, arithmetic and copies ran while one was open for 0% of the time, Pallas kernels for 13%

profile of v1, /device:TPU:2, one launch (start us, length us, event | category | flops | bytes accessed | tf_op | source)
XLA Modules:
  0.0 282.5 jit_solution(14063061269941752279)
XLA Ops:
  2.0 12.1 %all-to-all-start = ((s32[64,4,8]{2,1,0:T(4,128)}), s32[64,4,8]{2,1,0:T(4,128)S(1)}, u32[]{:S(2)}, u32[]{:S(2)}) async-start(s32[64,4,8]{2,1,0:T(4,128)} %fusion), calls=%async_computation | async-start | bytes 262144 | tf_op jit(solution)/shard_map/all_to_all | solution.py:581
  14.1 8.3 %tables.1 = (bf16[1280,512]{1,0:T(8,128)(2,1)S(1)}, bf16[2048,512]{1,0:T(8,128)(2,1)}) custom-call(bf16[1280,2048]{1,0:T(8,128)(2,1)} %refs_4_.1, f32[1,2048]{1,0:T(1,128)} %bitcast.9, bf16[2048,256]{1,0:T(8,128)(2,1)} %wk_hbm.1, bf16[2048,256]{1,0:T(8,128)(2,1)} %wv_hbm.1), custom_call_target="tpu_custom_call" | custom-call | flops 2684354560 | bytes 5242880 | tf_op jit(solution)/shard_map/tables/pallas_call | solution.py:81
  22.5 2.7 all-to-all-done
  26.4 3.1 %picked.1 = bf16[64,64,512]{2,1,0:T(8,128)(2,1)} custom-call(s32[64]{0:T(128)S(1)} %reduce_max.9.asked_ref, bf16[20,64,512]{2,1,0:T(8,128)(2,1)S(1)} %bitcast.8), custom_call_target="tpu_custom_call" | custom-call | tf_op jit(solution)/shard_map/picked/pallas_call | solution.py:149
  29.5 8.0 %all-to-all-start.1 = ((bf16[64,64,512]{2,1,0:T(8,128)(2,1)}), bf16[64,64,512]{2,1,0:T(8,128)(2,1)}, u32[]{:S(2)}, u32[]{:S(2)}) async-start(bf16[64,64,512]{2,1,0:T(8,128)(2,1)} %picked.1), calls=%async_computation.1 | async-start | bytes 8388608 | tf_op jit(solution)/shard_map/all_to_all | solution.py:586
  41.8 45.9 %collective-permute-done.2.refs_7_.refs_3_ = bf16[2048,512]{1,0:T(8,128)(2,1)S(1)} collective-permute-done((bf16[2048,512]{1,0:T(8,128)(2,1)S(1)}, bf16[2048,512]{1,0:T(8,128)(2,1)S(1)}, u32[]{:S(2)}, u32[]{:S(2)}) %collective-permute-start.2) | collective-permute-done | bytes 2097184 | tf_op jit(solution)/shard_map/ppermute | solution.py:559
  87.7 43.9 %collective-permute-done.1.refs_6_.refs_2_ = bf16[2048,512]{1,0:T(8,128)(2,1)S(1)} collective-permute-done((bf16[2048,512]{1,0:T(8,128)(2,1)S(1)}, bf16[2048,512]{1,0:T(8,128)(2,1)S(1)}, u32[]{:S(2)}, u32[]{:S(2)}) %collective-permute-start.1) | collective-permute-done | bytes 2097184 | tf_op jit(solution)/shard_map/ppermute | solution.py:559
  133.8 5.9 %value_slots.1 = bf16[64,64,256]{2,1,0:T(8,128)(2,1)} custom-call(s32[4,8]{1,0:T(4,128)S(1)} %bitcast.13, bf16[1024,256]{1,0:T(8,128)(2,1)} %q_ref.3, bf16[1024,256]{1,0:T(8,128)(2,1)} %g_ref.3, bf16[1024,256]{1,0:T(8,128)(2,1)} %c_ref.3, bf16[64,64,512]{2,1,0:T(8,128)(2,1)} %all-to-all-done.1.refs_0_.refs_1_.refs_2_.refs_3_.refs_4_.refs_5_.refs_6_.refs_7_, ...), custom_call_target="tpu_custom_call" | custom-call | flops 268435456 | bytes 6815744 | tf_op jit(solution)/shard_map/value_slots/pallas_call | solution.py:277
  139.6 9.6 %all-to-all-start.3 = ((bf16[64,64,256]{2,1,0:T(8,128)(2,1)}), bf16[64,64,256]{2,1,0:T(8,128)(2,1)S(1)}, u32[]{:S(2)}, u32[]{:S(2)}) async-start(bf16[64,64,256]{2,1,0:T(8,128)(2,1)} %value_slots.1), calls=%async_computation.3 | async-start | bytes 4194304 | tf_op jit(solution)/shard_map/all_to_all | solution.py:594
  149.3 7.7 %turned_normed.1.turned_hbm = bf16[2048,1280]{1,0:T(8,128)(2,1)} custom-call(bf16[1280,2048]{1,0:T(8,128)(2,1)} %refs_4_.1, f32[1,2048]{1,0:T(1,128)} %bitcast.10), custom_call_target="tpu_custom_call" | custom-call | flops 41943040 | bytes 10485760 | tf_op jit(solution)/shard_map/turned_normed/pallas_call | solution.py:119
  157.0 7.3 %key_slots.1 = (f32[1024,256]{1,0:T(8,128)}, bf16[64,64,256]{2,1,0:T(8,128)(2,1)}) custom-call(s32[4,8]{1,0:T(4,128)S(1)} %bitcast.14, bf16[1024,256]{1,0:T(8,128)(2,1)} %q_ref.3, bf16[1024,256]{1,0:T(8,128)(2,1)} %g_ref.3, bf16[1024,256]{1,0:T(8,128)(2,1)} %c_ref.3, ...), custom_call_target="tpu_custom_call" | custom-call | flops 536870912 | bytes 6815744 | tf_op jit(solution)/shard_map/key_slots/pallas_call | solution.py:277
  164.3 36.3 %all-to-all-done.3.back_ref = bf16[64,64,256]{2,1,0:T(8,128)(2,1)S(1)} async-done(((bf16[64,64,256]{2,1,0:T(8,128)(2,1)}), bf16[64,64,256]{2,1,0:T(8,128)(2,1)S(1)}, u32[]{:S(2)}, u32[]{:S(2)}) %all-to-all-start.3) | async-done | bytes 2097184 | tf_op jit(solution)/shard_map/all_to_all | solution.py:594
  200.6 5.8 %all-to-all-start.2 = ((bf16[64,64,256]{2,1,0:T(8,128)(2,1)}), bf16[64,64,256]{2,1,0:T(8,128)(2,1)}, u32[]{:S(2)}, u32[]{:S(2)}) async-start(bf16[64,64,256]{2,1,0:T(8,128)(2,1)} %get-tuple-element.48), calls=%async_computation.2 | async-start | bytes 4194304 | tf_op jit(solution)/shard_map/all_to_all | solution.py:601
  206.5 4.7 %value_sums.1 = (bf16[320,256]{1,0:T(8,128)(2,1)S(1)}, bf16[320,256]{1,0:T(8,128)(2,1)S(1)}, bf16[320,256]{1,0:T(8,128)(2,1)S(1)}, bf16[320,256]{1,0:T(8,128)(2,...) custom-call(s32[64]{0:T(128)S(1)} %reduce_max.9.asked_ref, s32[2]{0:T(128)S(1)} %pad_add_fusion.place_ref, ...), custom_call_target="tpu_custom_call" | custom-call | flops 1342177280 | bytes 5242880 | tf_op jit(solution)/shard_map/value_sums/pallas_call | solution.py:363
  213.4 2.9 %collective-permute-start.7 = (bf16[16,32,256]{2,1,0:T(8,128)(2,1)S(1)}, bf16[16,32,256]{2,1,0:T(8,128)(2,1)S(1)}, u32[]{:S(2)}, u32[]{:S(2)}) collective-permute-start(bf16[16,32,256]{2,1,0:T(8,128)(2,1)S(1)} %slice.59), channel_id=1, source_target_pairs={{0,16},{8,24},{16,0},{24,8},{1,17},{9,25},{17,1},{25,9},{2,18},{10... | collective-permute-start | bytes 786440 | tf_op jit(solution)/shard_map/ppermute | solution.py:566
  216.3 12.8 %collective-permute-done.7 = bf16[16,32,256]{2,1,0:T(8,128)(2,1)S(1)} collective-permute-done((bf16[16,32,256]{2,1,0:T(8,128)(2,1)S(1)}, bf16[16,32,256]{2,1,0:T(8,128)(2,1)S(1)}, u32[]{:S(2)}, u32[]{:S(2)}) %collective-permute-start.7) | collective-permute-done | bytes 262176 | tf_op jit(solution)/shard_map/ppermute | solution.py:566
  233.6 3.3 %collective-permute-done.8 = bf16[8,32,256]{2,1,0:T(8,128)(2,1)S(1)} collective-permute-done((bf16[8,32,256]{2,1,0:T(8,128)(2,1)S(1)}, bf16[8,32,256]{2,1,0:T(8,128)(2,1)S(1)}, u32[]{:S(2)}, u32[]{:S(2)}) %collective-permute-start.8) | collective-permute-done | bytes 131104 | tf_op jit(solution)/shard_map/ppermute | solution.py:566
  236.9 4.8 %collective-permute-start.9 = (f32[4,32,256]{2,1,0:T(8,128)S(1)}, f32[4,32,256]{2,1,0:T(8,128)S(1)}, u32[]{:S(2)}, u32[]{:S(2)}) collective-permute-start(f32[4,32,256]{2,1,0:T(8,128)S(1)} %slice.47), channel_id=1, source_target_pairs={{0,128},{32,160},{64,192},{96,224},{128,0},{160,32},{192,64},{224,... | collective-permute-start | bytes 393224 | tf_op jit(solution)/shard_map/ppermute | solution.py:566
  241.7 3.4 %near_products.1.near_ref = f32[320,2048]{1,0:T(8,128)S(1)} custom-call(bf16[320,256]{1,0:T(8,128)(2,1)S(1)} %get-tuple-element.52.refs_0_, bf16[320,256]{1,0:T(8,128)(2,1)S(1)} %collective-permute-done.3.refs_1_, bf16[320,256]{1,0:T(8,128)(2,1)S(1)} %collective-permute-done.4.refs_2_, bf16[320,256]{1,0:T(8,128)(2,1)S(1)} %collective-permute-done.5.refs_3_, ...), custom_call_target="tpu_custom_call" | custom-call | flops 1342177280 | bytes 4194304 | tf_op jit(solution)/shard_map/near_products/pallas_call | solution.py:446
  245.1 12.0 %all-to-all-done.2.back_ref = bf16[64,64,256]{2,1,0:T(8,128)(2,1)} async-done(((bf16[64,64,256]{2,1,0:T(8,128)(2,1)}), bf16[64,64,256]{2,1,0:T(8,128)(2,1)}, u32[]{:S(2)}, u32[]{:S(2)}) %all-to-all-start.2) | async-done | bytes 2097184 | tf_op jit(solution)/shard_map/all_to_all | solution.py:601
  259.5 3.4 %collective-permute-done.9 = f32[4,32,256]{2,1,0:T(8,128)S(1)} collective-permute-done((f32[4,32,256]{2,1,0:T(8,128)S(1)}, f32[4,32,256]{2,1,0:T(8,128)S(1)}, u32[]{:S(2)}, u32[]{:S(2)}) %collective-permute-start.9) | collective-permute-done | bytes 131104 | tf_op jit(solution)/shard_map/ppermute | solution.py:566
  263.7 5.3 %collective-permute-done.13 = f32[2,32,256]{2,1,0:T(8,128)S(1)} collective-permute-done((f32[2,32,256]{2,1,0:T(8,128)S(1)}, f32[2,32,256]{2,1,0:T(8,128)S(1)}, u32[]{:S(2)}, u32[]{:S(2)}) %collective-permute-start.13) | collective-permute-done | bytes 65568 | tf_op jit(solution)/shard_map/ppermute | solution.py:566
  273.3 3.2 %own_product.1 = (f32[320,2048]{1,0:T(8,128)S(1)}, bf16[320,2048]{1,0:T(8,128)(2,1)S(1)}, bf16[2048,256]{1,0:T(8,128)(2,1)S(1)}, bf16[2048,256]{1,0:T(8,128)(2,1)S(1)}, bf16[2048,256]{1,0:T(8,128)(2,1)S(1)}) custom-call(s32[2]{0:T(128)S(1)} %pad_add_fusion.place_ref, bf16[320,256]{1,0:T(8,128)(2,1)S(1)} %get-tuple-element.66.part_ref, ...), custom_call_target="tpu_custom_call" | custom-call | flops 335544320 | bytes 8388608 | tf_op jit(solution)/shard_map/own_product/pallas_call | solution.py:491
  279.0 3.4 %store_gradient.1 = f32[320,2048]{1,0:T(8,128)} custom-call(bf16[320,2048]{1,0:T(8,128)(2,1)S(1)} %get-tuple-element.68.rows_ref, f32[1,2048]{1,0:T(1,128)S(1)} %bitcast.11, f32[320,2048]{1,0:T(8,128)S(1)} %get-tuple-element.69.near_ref, bf16[320,256]{1,0:T(8,128)(2,1)S(1)} %collective-permute-done.10.refs_0_, ...), custom_call_target="tpu_custom_call" | custom-call | flops 1006632960 | bytes 2621440 | tf_op jit(solution)/shard_map/store_gradient/pallas_call | solution.py:539
  (48 shorter events, 25.7 us)
Async XLA Ops:
  2.0 23.1 %all-to-all-start = ((s32[64,4,8]{2,1,0:T(4,128)}), s32[64,4,8]{2,1,0:T(4,128)S(1)}, u32[]{:S(2)}, u32[]{:S(2)}) async-start(s32[64,4,8]{2,1,0:T(4,128)} %fusion), calls=%async_computation | async-start | bytes 262144 | tf_op jit(solution)/shard_map/all_to_all | solution.py:581
  29.5 8.0 %copy-start.2 = (bf16[2048,512]{1,0:T(8,128)(2,1)S(1)}, bf16[2048,512]{1,0:T(8,128)(2,1)}, u32[]{:S(2)}) copy-start(bf16[2048,512]{1,0:T(8,128)(2,1)} %get-tuple-element.42.refs_4_.refs_0_) | copy-start | bytes 6291460
  29.5 104.3 %copy-start.1 = (s32[8,4]{0,1:T(4,128)S(1)}, s32[8,4]{0,1:T(4,128)}, u32[]{:S(2)}) copy-start(s32[8,4]{0,1:T(4,128)} %param.16) | copy-start | bytes 388
  29.5 104.3 %all-to-all-start.1 = ((bf16[64,64,512]{2,1,0:T(8,128)(2,1)}), bf16[64,64,512]{2,1,0:T(8,128)(2,1)}, u32[]{:S(2)}, u32[]{:S(2)}) async-start(bf16[64,64,512]{2,1,0:T(8,128)(2,1)} %picked.1), calls=%async_computation.1 | async-start | bytes 8388608 | tf_op jit(solution)/shard_map/all_to_all | solution.py:586
  37.5 50.1 %collective-permute-start.2 = (bf16[2048,512]{1,0:T(8,128)(2,1)S(1)}, bf16[2048,512]{1,0:T(8,128)(2,1)S(1)}, u32[]{:S(2)}, u32[]{:S(2)}) collective-permute-start(bf16[2048,512]{1,0:T(8,128)(2,1)S(1)} %copy-done.2), channel_id=1, source_target_pairs={{0,2},{1,3},{2,0},{3,1},{4,6},{5,7},{6,4},{7,5},{8,10},{9,11},{10,... | collective-permute-start | bytes 6291464 | tf_op jit(solution)/shard_map/ppermute | solution.py:559
  39.7 91.8 %collective-permute-start.1 = (bf16[2048,512]{1,0:T(8,128)(2,1)S(1)}, bf16[2048,512]{1,0:T(8,128)(2,1)S(1)}, u32[]{:S(2)}, u32[]{:S(2)}) collective-permute-start(bf16[2048,512]{1,0:T(8,128)(2,1)S(1)} %copy-done.2), channel_id=1, source_target_pairs={{0,3},{1,0},{2,1},{3,2},{4,7},{5,4},{6,5},{7,6},{8,11},{9,8},{10,9... | collective-permute-start | bytes 6291464 | tf_op jit(solution)/shard_map/ppermute | solution.py:559
  41.2 91.8 %collective-permute-start = (bf16[2048,512]{1,0:T(8,128)(2,1)S(1)}, bf16[2048,512]{1,0:T(8,128)(2,1)}, u32[]{:S(2)}, u32[]{:S(2)}) collective-permute-start(bf16[2048,512]{1,0:T(8,128)(2,1)S(1)} %copy-done.2), channel_id=1, source_target_pairs={{0,1},{1,2},{2,3},{3,0},{4,5},{5,6},{6,7},{7,4},{8,9},{9,10},{10,1... | collective-permute-start | bytes 6291464 | tf_op jit(solution)/shard_map/ppermute | solution.py:559
  87.7 43.9 %copy-start.3 = (bf16[2048,512]{1,0:T(8,128)(2,1)}, bf16[2048,512]{1,0:T(8,128)(2,1)S(1)}, u32[]{:S(2)}) copy-start(bf16[2048,512]{1,0:T(8,128)(2,1)S(1)} %collective-permute-done.2.refs_7_.refs_3_) | copy-start | bytes 6291460
  131.6 1.4 copy-start.4
  139.6 61.0 %all-to-all-start.3 = ((bf16[64,64,256]{2,1,0:T(8,128)(2,1)}), bf16[64,64,256]{2,1,0:T(8,128)(2,1)S(1)}, u32[]{:S(2)}, u32[]{:S(2)}) async-start(bf16[64,64,256]{2,1,0:T(8,128)(2,1)} %value_slots.1), calls=%async_computation.3 | async-start | bytes 4194304 | tf_op jit(solution)/shard_map/all_to_all | solution.py:594
  200.6 56.5 %all-to-all-start.2 = ((bf16[64,64,256]{2,1,0:T(8,128)(2,1)}), bf16[64,64,256]{2,1,0:T(8,128)(2,1)}, u32[]{:S(2)}, u32[]{:S(2)}) async-start(bf16[64,64,256]{2,1,0:T(8,128)(2,1)} %get-tuple-element.48), calls=%async_computation.2 | async-start | bytes 4194304 | tf_op jit(solution)/shard_map/all_to_all | solution.py:601
  211.2 2.0 collective-permute-start.6
  213.4 15.7 %collective-permute-start.7 = (bf16[16,32,256]{2,1,0:T(8,128)(2,1)S(1)}, bf16[16,32,256]{2,1,0:T(8,128)(2,1)S(1)}, u32[]{:S(2)}, u32[]{:S(2)}) collective-permute-start(bf16[16,32,256]{2,1,0:T(8,128)(2,1)S(1)} %slice.59), channel_id=1, source_target_pairs={{0,16},{8,24},{16,0},{24,8},{1,17},{9,25},{17,1},{25,9},{2,18},{10... | collective-permute-start | bytes 786440 | tf_op jit(solution)/shard_map/ppermute | solution.py:566
  229.2 7.6 %collective-permute-start.8 = (bf16[8,32,256]{2,1,0:T(8,128)(2,1)S(1)}, bf16[8,32,256]{2,1,0:T(8,128)(2,1)S(1)}, u32[]{:S(2)}, u32[]{:S(2)}) collective-permute-start(bf16[8,32,256]{2,1,0:T(8,128)(2,1)S(1)} %slice.60), channel_id=1, source_target_pairs={{0,8},{8,0},{16,24},{24,16},{1,9},{9,1},{17,25},{25,17},{2,10},{10... | collective-permute-start | bytes 393224 | tf_op jit(solution)/shard_map/ppermute | solution.py:566
  229.3 12.3 %collective-permute-start.3 = (bf16[320,256]{1,0:T(8,128)(2,1)S(1)}, bf16[320,256]{1,0:T(8,128)(2,1)S(1)}, u32[]{:S(2)}, u32[]{:S(2)}) collective-permute-start(bf16[320,256]{1,0:T(8,128)(2,1)S(1)} %get-tuple-element.53), channel_id=1, source_target_pairs={{0,1},{1,2},{2,3},{3,0},{4,5},{5,6},{6,7},{7,4},{8,9},{9,10},{10,1... | collective-permute-start | bytes 491528 | tf_op jit(solution)/shard_map/ppermute | solution.py:559
  230.0 11.7 %collective-permute-start.4 = (bf16[320,256]{1,0:T(8,128)(2,1)S(1)}, bf16[320,256]{1,0:T(8,128)(2,1)S(1)}, u32[]{:S(2)}, u32[]{:S(2)}) collective-permute-start(bf16[320,256]{1,0:T(8,128)(2,1)S(1)} %get-tuple-element.54), channel_id=1, source_target_pairs={{0,3},{1,0},{2,1},{3,2},{4,7},{5,4},{6,5},{7,6},{8,11},{9,8},{10,9... | collective-permute-start | bytes 491528 | tf_op jit(solution)/shard_map/ppermute | solution.py:559
  231.4 10.2 %collective-permute-start.5 = (bf16[320,256]{1,0:T(8,128)(2,1)S(1)}, bf16[320,256]{1,0:T(8,128)(2,1)S(1)}, u32[]{:S(2)}, u32[]{:S(2)}) collective-permute-start(bf16[320,256]{1,0:T(8,128)(2,1)S(1)} %get-tuple-element.55), channel_id=1, source_target_pairs={{0,2},{1,3},{2,0},{3,1},{4,6},{5,7},{6,4},{7,5},{8,10},{9,11},{10,... | collective-permute-start | bytes 491528 | tf_op jit(solution)/shard_map/ppermute | solution.py:559
  236.9 26.1 %collective-permute-start.9 = (f32[4,32,256]{2,1,0:T(8,128)S(1)}, f32[4,32,256]{2,1,0:T(8,128)S(1)}, u32[]{:S(2)}, u32[]{:S(2)}) collective-permute-start(f32[4,32,256]{2,1,0:T(8,128)S(1)} %slice.47), channel_id=1, source_target_pairs={{0,128},{32,160},{64,192},{96,224},{128,0},{160,32},{192,64},{224,... | collective-permute-start | bytes 393224 | tf_op jit(solution)/shard_map/ppermute | solution.py:566
  262.9 6.0 %collective-permute-start.13 = (f32[2,32,256]{2,1,0:T(8,128)S(1)}, f32[2,32,256]{2,1,0:T(8,128)S(1)}, u32[]{:S(2)}, u32[]{:S(2)}) collective-permute-start(f32[2,32,256]{2,1,0:T(8,128)S(1)} %slice.39), channel_id=1, source_target_pairs={{0,64},{32,96},{64,0},{96,32},{128,192},{160,224},{192,128},{224,1... | collective-permute-start | bytes 196616 | tf_op jit(solution)/shard_map/ppermute | solution.py:566
  268.9 10.0 %copy-start = (f32[2048]{0:T(1024)S(1)}, f32[2048]{0:T(1024)}, u32[]{:S(2)}) copy-start(f32[2048]{0:T(1024)} %param.13) | copy-start | bytes 24580
  269.0 7.5 %collective-permute-start.14 = (f32[1,32,256]{2,1,0:T(8,128)S(1)}, f32[1,32,256]{2,1,0:T(8,128)S(1)}, u32[]{:S(2)}, u32[]{:S(2)}) collective-permute-start(f32[1,32,256]{2,1,0:T(8,128)S(1)} %slice.49), channel_id=1, source_target_pairs={{0,32},{32,0},{64,96},{96,64},{128,160},{160,128},{192,224},{224,1... | collective-permute-start | bytes 98312 | tf_op jit(solution)/shard_map/ppermute | solution.py:566
  269.1 8.0 %collective-permute-start.10 = (bf16[320,256]{1,0:T(8,128)(2,1)S(1)}, bf16[320,256]{1,0:T(8,128)(2,1)S(1)}, u32[]{:S(2)}, u32[]{:S(2)}) collective-permute-start(bf16[320,256]{1,0:T(8,128)(2,1)S(1)} %get-tuple-element.70), channel_id=1, source_target_pairs={{0,1},{1,2},{2,3},{3,0},{4,5},{5,6},{6,7},{7,4},{8,9},{9,10},{10,1... | collective-permute-start | bytes 491528 | tf_op jit(solution)/shard_map/ppermute | solution.py:559
  269.7 7.4 %collective-permute-start.11 = (bf16[320,256]{1,0:T(8,128)(2,1)S(1)}, bf16[320,256]{1,0:T(8,128)(2,1)S(1)}, u32[]{:S(2)}, u32[]{:S(2)}) collective-permute-start(bf16[320,256]{1,0:T(8,128)(2,1)S(1)} %get-tuple-element.71), channel_id=1, source_target_pairs={{0,3},{1,0},{2,1},{3,2},{4,7},{5,4},{6,5},{7,6},{8,11},{9,8},{10,9... | collective-permute-start | bytes 491528 | tf_op jit(solution)/shard_map/ppermute | solution.py:559
  271.2 7.8 %collective-permute-start.12 = (bf16[320,256]{1,0:T(8,128)(2,1)S(1)}, bf16[320,256]{1,0:T(8,128)(2,1)S(1)}, u32[]{:S(2)}, u32[]{:S(2)}) collective-permute-start(bf16[320,256]{1,0:T(8,128)(2,1)S(1)} %get-tuple-element.72), channel_id=1, source_target_pairs={{0,2},{1,3},{2,0},{3,1},{4,6},{5,7},{6,4},{7,5},{8,10},{9,11},{10,... | collective-permute-start | bytes 491528 | tf_op jit(solution)/shard_map/ppermute | solution.py:559

commit v2 on v1

--- a/solution.py
+++ b/solution.py
@@ -586,20 +586,23 @@
     got = lax.all_to_all(picked, ST, split_axis=0, concat_axis=0, tiled=True)
 
     both, _ = lax.optimization_barrier((both, picked))
-    weights = [both] + [shifted(both, turn) for turn in (1, 3, 2)]
-    got, *came = lax.optimization_barrier((got, *weights[1:]))
-    weights = [both] + came
+    weights = [both]
+    for turn in (1, 3, 2):
+        weights.append(shifted(both, turn))
 
     (outgoing,) = attention(owner_turned, queries, gate_pre, cotangent, got, True)
     back_values = lax.all_to_all(outgoing, ST, split_axis=0, concat_axis=0, tiled=True)
-    late_store, late_got, _ = lax.optimization_barrier((store, got, outgoing))
+    late_got, _ = lax.optimization_barrier((got, outgoing))
     grad_queries, outgoing = attention(
         owner_turned, queries, gate_pre, cotangent, late_got, False
     )
-    turned = turned_normed(late_store, gain)
+    turned = turned_normed(store, gain)
     outgoing, turned = lax.optimization_barrier((outgoing, turned))
     back_keys = lax.all_to_all(outgoing, ST, split_axis=0, concat_axis=0, tiled=True)
-    back_values, turned, _ = lax.optimization_barrier((back_values, turned, grad_queries))
+    back_values, turned, *near_weights = lax.optimization_barrier(
+        (back_values, turned, *weights[1:])
+    )
+    weights[1:] = near_weights
 
     own, first, second, third, mine, other = value_sums(
         asked, place, back_values, turned, passages, st_size
@@ -611,19 +614,17 @@
     terms = halved(terms, "st_1", 2, jnp.bfloat16)
     terms = halved(terms, "st_1", 1, jnp.bfloat16)
     back_keys, near = lax.optimization_barrier((back_keys, near))
-    terms = halved(terms, "st_0", 4, jnp.float32)
+    spread = [terms[0]]
+    for distance in range(1, terms.shape[0]):
+        pairs = [(i, i ^ distance) for i in range(terms.shape[0])]
+        spread.append(lax.ppermute(terms[distance], "st_0", pairs))
 
     own, first, second, third = key_sums(asked, place, back_keys, passages)
-    own, first, second, third, terms = lax.optimization_barrier(
-        (own, first, second, third, terms)
-    )
     parts = []
     for part, turn in ((first, 1), (third, 3), (second, 2)):
         parts.append(shifted(part, turn))
     near, own_rows, *key_weights = own_product(place, own, near, weights, store)
-    terms = halved(terms, "st_0", 2, jnp.float32)
-    terms = halved(terms, "st_0", 1, jnp.float32)
-    grad_w_value = terms.reshape(terms.shape[1:])
+    grad_w_value = sum(spread)
     grad_store = store_gradient(own_rows, gain, near, parts, key_weights)
     return (grad_queries, grad_store, grad_w_value)
 

time: 284 us -> 351 us (1.24)
  blocking collectives: 0 us -> 104 us
  waiting for transfers between devices: 170 us -> 137 us
    all_to_all x0 -> x1, blocking collectives: none -> 104 us  [local(): got = lax.all_to_all(picked, ST, split_axis=0, concat_axis=0, tiled=True)]
    ppermute x5 -> x2, waiting for transfers between devices: 24.8 us -> 2.63 us  [halved(): came = lax.ppermute(value[half:].astype(kind), axis, pairs)]
    ppermute x0 -> x7, starting transfers between devices: none -> 14.5 us  [local(): spread.append(lax.ppermute(terms[distance], 'st_0', pairs))]
    all_to_all x2, waiting for transfers between devices: 48.3 us -> 36.3 us  [local(): lax.all_to_all(outgoing, ST, split_axis=0, concat_axis=0, tiled=True)]
    all_to_all x1 -> x0, starting transfers between devices: 8.01 us -> none  [local(): got = lax.all_to_all(picked, ST, split_axis=0, concat_axis=0, tiled=True)]
    all_to_all x2, starting transfers between devices: 15.4 us -> 11 us  [local(): lax.all_to_all(outgoing, ST, split_axis=0, concat_axis=0, tiled=True)]
    ppermute x5 -> x2, starting transfers between devices: 8.62 us -> 4.95 us  [halved(): came = lax.ppermute(value[half:].astype(kind), axis, pairs)]
  transfers between devices with their start and end apart: 19 -> 22, of which waited for: 12 -> 9; matrix products, arithmetic and copies ran while one was open for 0% -> 0% of each run, Pallas kernels for 13% -> 11%
where the time goes in v2:
time: 351 us; the launch traced here: 350 us
  waiting for transfers between devices  137 us (39%)
  blocking collectives  104 us (30%)
  starting transfers between devices  54.8 us (16%)
  Pallas kernels  49.1 us (14%)
  other arithmetic  3.58 us (1%)
    all_to_all x1, blocking collectives, local(): got = lax.all_to_all(picked, ST, split_axis=0, concat_axis=0, tiled=True)  104 us
    ppermute x9, waiting for transfers between devices, shifted(): return lax.ppermute(value, 'tp', [(i, (i + turn) % 4) for i in range(4)])  92.8 us
    all_to_all x2, waiting for transfers between devices, local(): lax.all_to_all(outgoing, ST, split_axis=0, concat_axis=0, tiled=True)  36.3 us
    ppermute x7, starting transfers between devices, local(): spread.append(lax.ppermute(terms[distance], 'st_0', pairs))  14.5 us
    pallas_call x2, Pallas kernels, attention(): pl.pallas_call(value_slots_kernel if keys_only else key_slots_kernel, gri...  13.1 us
    ppermute x9, starting transfers between devices, shifted(): return lax.ppermute(value, 'tp', [(i, (i + turn) % 4) for i in range(4)])  12.2 us
    all_to_all x1, starting transfers between devices, local(): lax.all_to_all(requests, ST, split_axis=0, concat_axis=0, tiled=True)  12.1 us
    all_to_all x2, starting transfers between devices, local(): lax.all_to_all(outgoing, ST, split_axis=0, concat_axis=0, tiled=True)  11 us
  transfers between devices with their start and end apart: 22, of which 9 were waited for; matrix products, arithmetic and copies ran while one was open for 0% of the time, Pallas kernels for 11%

profile of v2, /device:TPU:2, one launch (start us, length us, event | category | flops | bytes accessed | tf_op | source)
XLA Modules:
  0.0 349.9 jit_solution(2557864010637486641)
XLA Ops:
  2.0 12.1 %all-to-all-start = ((s32[64,4,8]{2,1,0:T(4,128)}), s32[64,4,8]{2,1,0:T(4,128)S(1)}, u32[]{:S(2)}, u32[]{:S(2)}) async-start(s32[64,4,8]{2,1,0:T(4,128)} %fusion), calls=%async_computation | async-start | bytes 262144 | tf_op jit(solution)/shard_map/all_to_all | solution.py:581
  14.1 8.3 %tables.1 = (bf16[1280,512]{1,0:T(8,128)(2,1)S(1)}, bf16[2048,512]{1,0:T(8,128)(2,1)}) custom-call(bf16[1280,2048]{1,0:T(8,128)(2,1)} %refs_4_.1, f32[1,2048]{1,0:T(1,128)} %bitcast.37, bf16[2048,256]{1,0:T(8,128)(2,1)} %wk_hbm.1, bf16[2048,256]{1,0:T(8,128)(2,1)} %wv_hbm.1), custom_call_target="tpu_custom_call" | custom-call | flops 2684354560 | bytes 5242880 | tf_op jit(solution)/shard_map/tables/pallas_call | solution.py:81
  22.5 2.7 all-to-all-done
  26.4 3.1 picked.1
  29.5 104.0 %all_to_all.20.refs_0_.refs_1_.refs_2_.refs_3_.refs_4_.refs_5_.refs_6_.refs_7_ = bf16[64,64,512]{2,1,0:T(8,128)(2,1)} all-to-all(bf16[64,64,512]{2,1,0:T(8,128)(2,1)} %picked.1), channel_id=1, replica_groups=mesh['st_0'=8,'st_1'=4,'st_2'=2,'tp'=4] {'st_0','st_1','st_2'}, dimensions={0} | all-to-all | bytes 8388608 | tf_op jit(solution)/shard_map/all_to_all | solution.py:586
  133.5 5.8 %value_slots.1 = bf16[64,64,256]{2,1,0:T(8,128)(2,1)} custom-call(s32[4,8]{1,0:T(4,128)S(1)} %bitcast.41, bf16[1024,256]{1,0:T(8,128)(2,1)} %q_ref.3, bf16[1024,256]{1,0:T(8,128)(2,1)} %g_ref.3, bf16[1024,256]{1,0:T(8,128)(2,1)} %c_ref.3, bf16[64,64,512]{2,1,0:T(8,128)(2,1)} %all_to_all.20.refs_0_.refs_1_.refs_2_.refs_3_.refs_4_.refs_5_.refs_6_.refs_7_, ...), custom_call_target="tpu_custom_call" | custom-call | flops 268435456 | bytes 6815744 | tf_op jit(solution)/shard_map/value_slots/pallas_call | solution.py:277
  139.3 5.4 %all-to-all-start.3 = ((bf16[64,64,256]{2,1,0:T(8,128)(2,1)}), bf16[64,64,256]{2,1,0:T(8,128)(2,1)S(1)}, u32[]{:S(2)}, u32[]{:S(2)}) async-start(bf16[64,64,256]{2,1,0:T(8,128)(2,1)} %value_slots.1), calls=%async_computation.3 | async-start | bytes 4194304 | tf_op jit(solution)/shard_map/all_to_all | solution.py:594
  144.7 7.7 %turned_normed.1.turned_hbm = bf16[2048,1280]{1,0:T(8,128)(2,1)} custom-call(bf16[1280,2048]{1,0:T(8,128)(2,1)} %refs_4_.1, f32[1,2048]{1,0:T(1,128)} %bitcast.38), custom_call_target="tpu_custom_call" | custom-call | flops 41943040 | bytes 10485760 | tf_op jit(solution)/shard_map/turned_normed/pallas_call | solution.py:119
  152.4 7.3 %key_slots.1 = (f32[1024,256]{1,0:T(8,128)}, bf16[64,64,256]{2,1,0:T(8,128)(2,1)}) custom-call(s32[4,8]{1,0:T(4,128)S(1)} %bitcast.42, bf16[1024,256]{1,0:T(8,128)(2,1)} %q_ref.3, bf16[1024,256]{1,0:T(8,128)(2,1)} %g_ref.3, bf16[1024,256]{1,0:T(8,128)(2,1)} %c_ref.3, ...), custom_call_target="tpu_custom_call" | custom-call | flops 536870912 | bytes 6815744 | tf_op jit(solution)/shard_map/key_slots/pallas_call | solution.py:277
  159.7 36.3 %all-to-all-done.3.back_ref = bf16[64,64,256]{2,1,0:T(8,128)(2,1)S(1)} async-done(((bf16[64,64,256]{2,1,0:T(8,128)(2,1)}), bf16[64,64,256]{2,1,0:T(8,128)(2,1)S(1)}, u32[]{:S(2)}, u32[]{:S(2)}) %all-to-all-start.3) | async-done | bytes 2097184 | tf_op jit(solution)/shard_map/all_to_all | solution.py:594
  196.0 5.6 %all-to-all-start.2 = ((bf16[64,64,256]{2,1,0:T(8,128)(2,1)}), bf16[64,64,256]{2,1,0:T(8,128)(2,1)}, u32[]{:S(2)}, u32[]{:S(2)}) async-start(bf16[64,64,256]{2,1,0:T(8,128)(2,1)} %get-tuple-element.37), calls=%async_computation.2 | async-start | bytes 4194304 | tf_op jit(solution)/shard_map/all_to_all | solution.py:601
  206.0 46.1 %collective-permute-done.2.refs_7_.refs_3_ = bf16[2048,512]{1,0:T(8,128)(2,1)} collective-permute-done((bf16[2048,512]{1,0:T(8,128)(2,1)}, bf16[2048,512]{1,0:T(8,128)(2,1)}, u32[]{:S(2)}, u32[]{:S(2)}) %collective-permute-start.2) | collective-permute-done | bytes 2097184 | tf_op jit(solution)/shard_map/ppermute | solution.py:559
  252.1 43.9 %collective-permute-done.1.refs_6_.refs_2_ = bf16[2048,512]{1,0:T(8,128)(2,1)} collective-permute-done((bf16[2048,512]{1,0:T(8,128)(2,1)}, bf16[2048,512]{1,0:T(8,128)(2,1)}, u32[]{:S(2)}, u32[]{:S(2)}) %collective-permute-start.1) | collective-permute-done | bytes 2097184 | tf_op jit(solution)/shard_map/ppermute | solution.py:559
  296.1 4.7 %value_sums.1 = (bf16[320,256]{1,0:T(8,128)(2,1)S(1)}, bf16[320,256]{1,0:T(8,128)(2,1)S(1)}, bf16[320,256]{1,0:T(8,128)(2,1)S(1)}, bf16[320,256]{1,0:T(8,128)(2,...) custom-call(s32[64]{0:T(128)S(1)} %reduce_max.9.asked_ref, s32[2]{0:T(128)S(1)} %pad_add_fusion.place_ref, ...), custom_call_target="tpu_custom_call" | custom-call | flops 1342177280 | bytes 5242880 | tf_op jit(solution)/shard_map/value_sums/pallas_call | solution.py:363
  303.0 3.2 collective-permute-start.10
  310.3 2.6 collective-permute-done.10
  314.7 2.7 collective-permute-done.5.refs_3_
  317.5 3.4 near_products.1.near_ref
  320.9 2.4 key_sums.1
  328.8 2.9 collective-permute-start.18
  331.7 3.2 own_product.1
  336.4 3.8 %collective-permute-start.16 = (f32[32,256]{1,0:T(8,128)S(1)}, f32[32,256]{1,0:T(8,128)S(1)}, u32[]{:S(2)}, u32[]{:S(2)}) collective-permute-start(f32[32,256]{1,0:T(8,128)S(1)} %get-tuple-element.66), channel_id=1, source_target_pairs={{0,160},{32,128},{64,224},{96,192},{128,32},{160,0},{192,96},{224,... | collective-permute-start | bytes 98312 | tf_op jit(solution)/shard_map/ppermute | solution.py:620
  342.0 2.4 collective-permute-start.14
  344.9 3.2 store_gradient.1
  (45 shorter events, 26.2 us)
Async XLA Ops:
  2.0 23.1 %all-to-all-start = ((s32[64,4,8]{2,1,0:T(4,128)}), s32[64,4,8]{2,1,0:T(4,128)S(1)}, u32[]{:S(2)}, u32[]{:S(2)}) async-start(s32[64,4,8]{2,1,0:T(4,128)} %fusion), calls=%async_computation | async-start | bytes 262144 | tf_op jit(solution)/shard_map/all_to_all | solution.py:581
  29.5 104.0 %copy-start.1 = (s32[8,4]{0,1:T(4,128)S(1)}, s32[8,4]{0,1:T(4,128)}, u32[]{:S(2)}) copy-start(s32[8,4]{0,1:T(4,128)} %param.16) | copy-start | bytes 388
  139.3 56.7 %all-to-all-start.3 = ((bf16[64,64,256]{2,1,0:T(8,128)(2,1)}), bf16[64,64,256]{2,1,0:T(8,128)(2,1)S(1)}, u32[]{:S(2)}, u32[]{:S(2)}) async-start(bf16[64,64,256]{2,1,0:T(8,128)(2,1)} %value_slots.1), calls=%async_computation.3 | async-start | bytes 4194304 | tf_op jit(solution)/shard_map/all_to_all | solution.py:594
  196.0 124.8 %all-to-all-start.2 = ((bf16[64,64,256]{2,1,0:T(8,128)(2,1)}), bf16[64,64,256]{2,1,0:T(8,128)(2,1)}, u32[]{:S(2)}, u32[]{:S(2)}) async-start(bf16[64,64,256]{2,1,0:T(8,128)(2,1)} %get-tuple-element.37), calls=%async_computation.2 | async-start | bytes 4194304 | tf_op jit(solution)/shard_map/all_to_all | solution.py:601
  201.6 50.5 %collective-permute-start.2 = (bf16[2048,512]{1,0:T(8,128)(2,1)}, bf16[2048,512]{1,0:T(8,128)(2,1)}, u32[]{:S(2)}, u32[]{:S(2)}) collective-permute-start(bf16[2048,512]{1,0:T(8,128)(2,1)} %get-tuple-element.40.refs_4_.refs_0_), channel_id=1, source_target_pairs={{0,2},{1,3},{2,0},{3,1},{4,6},{5,7},{6,4},{7,5},{8,10},{9,11},{10,... | collective-permute-start | bytes 6291464 | tf_op jit(solution)/shard_map/ppermute | solution.py:559
  203.9 92.2 %collective-permute-start.1 = (bf16[2048,512]{1,0:T(8,128)(2,1)}, bf16[2048,512]{1,0:T(8,128)(2,1)}, u32[]{:S(2)}, u32[]{:S(2)}) collective-permute-start(bf16[2048,512]{1,0:T(8,128)(2,1)} %get-tuple-element.40.refs_4_.refs_0_), channel_id=1, source_target_pairs={{0,3},{1,0},{2,1},{3,2},{4,7},{5,4},{6,5},{7,6},{8,11},{9,8},{10,9... | collective-permute-start | bytes 6291464 | tf_op jit(solution)/shard_map/ppermute | solution.py:559
  205.3 90.8 %collective-permute-start = (bf16[2048,512]{1,0:T(8,128)(2,1)}, bf16[2048,512]{1,0:T(8,128)(2,1)}, u32[]{:S(2)}, u32[]{:S(2)}) collective-permute-start(bf16[2048,512]{1,0:T(8,128)(2,1)} %get-tuple-element.40.refs_4_.refs_0_), channel_id=1, source_target_pairs={{0,1},{1,2},{2,3},{3,0},{4,5},{5,6},{6,7},{7,4},{8,9},{9,10},{10,1... | collective-permute-start | bytes 6291464 | tf_op jit(solution)/shard_map/ppermute | solution.py:559
  300.8 2.0 collective-permute-start.9
  303.0 9.9 %collective-permute-start.10 = (bf16[16,32,256]{2,1,0:T(8,128)(2,1)S(1)}, bf16[16,32,256]{2,1,0:T(8,128)(2,1)S(1)}, u32[]{:S(2)}, u32[]{:S(2)}) collective-permute-start(bf16[16,32,256]{2,1,0:T(8,128)(2,1)S(1)} %slice.88), channel_id=1, source_target_pairs={{0,16},{8,24},{16,0},{24,8},{1,17},{9,25},{17,1},{25,9},{2,18},{10... | collective-permute-start | bytes 786440 | tf_op jit(solution)/shard_map/ppermute | solution.py:566
  306.2 8.5 %collective-permute-start.3 = (bf16[320,256]{1,0:T(8,128)(2,1)S(1)}, bf16[320,256]{1,0:T(8,128)(2,1)S(1)}, u32[]{:S(2)}, u32[]{:S(2)}) collective-permute-start(bf16[320,256]{1,0:T(8,128)(2,1)S(1)} %get-tuple-element.44), channel_id=1, source_target_pairs={{0,1},{1,2},{2,3},{3,0},{4,5},{5,6},{6,7},{7,4},{8,9},{9,10},{10,1... | collective-permute-start | bytes 491528 | tf_op jit(solution)/shard_map/ppermute | solution.py:559
  307.6 7.1 %collective-permute-start.4 = (bf16[320,256]{1,0:T(8,128)(2,1)S(1)}, bf16[320,256]{1,0:T(8,128)(2,1)S(1)}, u32[]{:S(2)}, u32[]{:S(2)}) collective-permute-start(bf16[320,256]{1,0:T(8,128)(2,1)S(1)} %get-tuple-element.45), channel_id=1, source_target_pairs={{0,3},{1,0},{2,1},{3,2},{4,7},{5,4},{6,5},{7,6},{8,11},{9,8},{10,9... | collective-permute-start | bytes 491528 | tf_op jit(solution)/shard_map/ppermute | solution.py:559
  308.2 9.2 %collective-permute-start.5 = (bf16[320,256]{1,0:T(8,128)(2,1)S(1)}, bf16[320,256]{1,0:T(8,128)(2,1)S(1)}, u32[]{:S(2)}, u32[]{:S(2)}) collective-permute-start(bf16[320,256]{1,0:T(8,128)(2,1)S(1)} %get-tuple-element.46), channel_id=1, source_target_pairs={{0,2},{1,3},{2,0},{3,1},{4,6},{5,7},{6,4},{7,5},{8,10},{9,11},{10,... | collective-permute-start | bytes 491528 | tf_op jit(solution)/shard_map/ppermute | solution.py:559
  313.0 14.2 %collective-permute-start.11 = (bf16[8,32,256]{2,1,0:T(8,128)(2,1)S(1)}, bf16[8,32,256]{2,1,0:T(8,128)(2,1)S(1)}, u32[]{:S(2)}, u32[]{:S(2)}) collective-permute-start(bf16[8,32,256]{2,1,0:T(8,128)(2,1)S(1)} %slice.89), channel_id=1, source_target_pairs={{0,8},{8,0},{16,24},{24,16},{1,9},{9,1},{17,25},{25,17},{2,10},{10... | collective-permute-start | bytes 393224 | tf_op jit(solution)/shard_map/ppermute | solution.py:566
  323.3 11.6 %collective-permute-start.6 = (bf16[320,256]{1,0:T(8,128)(2,1)S(1)}, bf16[320,256]{1,0:T(8,128)(2,1)S(1)}, u32[]{:S(2)}, u32[]{:S(2)}) collective-permute-start(bf16[320,256]{1,0:T(8,128)(2,1)S(1)} %get-tuple-element.55), channel_id=1, source_target_pairs={{0,1},{1,2},{2,3},{3,0},{4,5},{5,6},{6,7},{7,4},{8,9},{9,10},{10,1... | collective-permute-start | bytes 491528 | tf_op jit(solution)/shard_map/ppermute | solution.py:559
  323.4 13.1 %collective-permute-start.7 = (bf16[320,256]{1,0:T(8,128)(2,1)S(1)}, bf16[320,256]{1,0:T(8,128)(2,1)S(1)}, u32[]{:S(2)}, u32[]{:S(2)}) collective-permute-start(bf16[320,256]{1,0:T(8,128)(2,1)S(1)} %get-tuple-element.56), channel_id=1, source_target_pairs={{0,3},{1,0},{2,1},{3,2},{4,7},{5,4},{6,5},{7,6},{8,11},{9,8},{10,9... | collective-permute-start | bytes 491528 | tf_op jit(solution)/shard_map/ppermute | solution.py:559
  325.4 14.8 %collective-permute-start.8 = (bf16[320,256]{1,0:T(8,128)(2,1)S(1)}, bf16[320,256]{1,0:T(8,128)(2,1)S(1)}, u32[]{:S(2)}, u32[]{:S(2)}) collective-permute-start(bf16[320,256]{1,0:T(8,128)(2,1)S(1)} %get-tuple-element.57), channel_id=1, source_target_pairs={{0,2},{1,3},{2,0},{3,1},{4,6},{5,7},{6,4},{7,5},{8,10},{9,11},{10,... | collective-permute-start | bytes 491528 | tf_op jit(solution)/shard_map/ppermute | solution.py:559
  327.2 14.8 %collective-permute-start.12 = (f32[32,256]{1,0:T(8,128)S(1)}, f32[32,256]{1,0:T(8,128)S(1)}, u32[]{:S(2)}, u32[]{:S(2)}) collective-permute-start(f32[32,256]{1,0:T(8,128)S(1)} %get-tuple-element.63), channel_id=1, source_target_pairs={{0,32},{32,0},{64,96},{96,64},{128,160},{160,128},{192,224},{224,1... | collective-permute-start | bytes 98312 | tf_op jit(solution)/shard_map/ppermute | solution.py:620
  328.8 15.6 %collective-permute-start.18 = (f32[32,256]{1,0:T(8,128)S(1)}, f32[32,256]{1,0:T(8,128)S(1)}, u32[]{:S(2)}, u32[]{:S(2)}) collective-permute-start(f32[32,256]{1,0:T(8,128)S(1)} %get-tuple-element.64), channel_id=1, source_target_pairs={{0,224},{32,192},{64,160},{96,128},{128,96},{160,64},{192,32},{224... | collective-permute-start | bytes 98312 | tf_op jit(solution)/shard_map/ppermute | solution.py:620
  331.7 13.2 %copy-start = (f32[2048]{0:T(1024)S(1)}, f32[2048]{0:T(1024)}, u32[]{:S(2)}) copy-start(f32[2048]{0:T(1024)} %param.13) | copy-start | bytes 24580
  334.9 13.3 %collective-permute-start.17 = (f32[32,256]{1,0:T(8,128)S(1)}, f32[32,256]{1,0:T(8,128)S(1)}, u32[]{:S(2)}, u32[]{:S(2)}) collective-permute-start(f32[32,256]{1,0:T(8,128)S(1)} %get-tuple-element.65), channel_id=1, source_target_pairs={{0,192},{32,224},{64,128},{96,160},{128,64},{160,96},{192,0},{224,... | collective-permute-start | bytes 98312 | tf_op jit(solution)/shard_map/ppermute | solution.py:620
  336.4 11.7 %collective-permute-start.16 = (f32[32,256]{1,0:T(8,128)S(1)}, f32[32,256]{1,0:T(8,128)S(1)}, u32[]{:S(2)}, u32[]{:S(2)}) collective-permute-start(f32[32,256]{1,0:T(8,128)S(1)} %get-tuple-element.66), channel_id=1, source_target_pairs={{0,160},{32,128},{64,224},{96,192},{128,32},{160,0},{192,96},{224,... | collective-permute-start | bytes 98312 | tf_op jit(solution)/shard_map/ppermute | solution.py:620
  340.2 8.0 %collective-permute-start.15 = (f32[32,256]{1,0:T(8,128)S(1)}, f32[32,256]{1,0:T(8,128)S(1)}, u32[]{:S(2)}, u32[]{:S(2)}) collective-permute-start(f32[32,256]{1,0:T(8,128)S(1)} %get-tuple-element.67), channel_id=1, source_target_pairs={{0,128},{32,160},{64,192},{96,224},{128,0},{160,32},{192,64},{224,... | collective-permute-start | bytes 98312 | tf_op jit(solution)/shard_map/ppermute | solution.py:620
  342.0 6.1 %collective-permute-start.14 = (f32[32,256]{1,0:T(8,128)S(1)}, f32[32,256]{1,0:T(8,128)S(1)}, u32[]{:S(2)}, u32[]{:S(2)}) collective-permute-start(f32[32,256]{1,0:T(8,128)S(1)} %get-tuple-element.68), channel_id=1, source_target_pairs={{0,96},{32,64},{64,32},{96,0},{128,224},{160,192},{192,160},{224,1... | collective-permute-start | bytes 98312 | tf_op jit(solution)/shard_map/ppermute | solution.py:620
  344.4 4.8 %collective-permute-start.13 = (f32[32,256]{1,0:T(8,128)S(1)}, f32[32,256]{1,0:T(8,128)S(1)}, u32[]{:S(2)}, u32[]{:S(2)}) collective-permute-start(f32[32,256]{1,0:T(8,128)S(1)} %get-tuple-element.69), channel_id=1, source_target_pairs={{0,64},{32,96},{64,0},{96,32},{128,192},{160,224},{192,128},{224,1... | collective-permute-start | bytes 98312 | tf_op jit(solution)/shard_map/ppermute | solution.py:620

commit v3 on v2

--- a/solution.py
+++ b/solution.py
@@ -158,6 +158,28 @@
         compiler_params=pltpu.CompilerParams(vmem_limit_bytes=8 * MIB),
         name="picked",
     )(asked, table)
+
+
+def gated_kernel(g_ref, c_ref, out_ref):
+    gate = jax.nn.sigmoid(g_ref[...].astype(jnp.float32))
+    out_ref[...] = (gate * c_ref[...].astype(jnp.float32)).astype(jnp.bfloat16)
+
+
+def gated(gate_pre, cotangent):
+    rows, width = gate_pre.shape
+    step = pl.BlockSpec((rows // 4, width), lambda i: (i, 0))
+    return pl.pallas_call(
+        gated_kernel,
+        grid=(4,),
+        in_specs=[step, step],
+        out_specs=step,
+        out_shape=jax.ShapeDtypeStruct((rows, width), jnp.bfloat16),
+        compiler_params=params(8),
+        cost_estimate=pl.CostEstimate(
+            flops=8 * rows * width, bytes_accessed=6 * rows * width, transcendentals=rows * width
+        ),
+        name="gated",
+    )(in_hbm(gate_pre), in_hbm(cotangent))
 
 
 def slot_copies(owner_ref, scratch, out_hbm, sems, at, parity):
@@ -197,59 +219,90 @@
             copy.wait()
 
 
-def block_units(owner_ref, q_ref, g_ref, c_ref, pieces):
+def softmax_turned(keys, q):
+    scores = dot_nt(keys, q) * HD ** (-0.5)
+    weights = jnp.exp(scores - jnp.max(scores, axis=0, keepdims=True))
+    return weights * (1.0 / jnp.sum(weights, axis=0, keepdims=True))
+
+
+def value_slots_kernel(owner_ref, q_ref, gin_ref, got_hbm, out_hbm, keys_ref, made_ref, sems):
+    per_block, blocks = owner_ref.shape
+    length = q_ref.shape[0] // blocks
     width = q_ref.shape[1]
+    places = [(b, j) for b in range(blocks) for j in range(per_block)]
+    arrivals, sent = [], []
+    for i, (b, j) in enumerate(places):
+        piece = got_hbm.at[owner_ref[j, b], :, :width]
+        arrivals.append(pltpu.make_async_copy(piece, keys_ref.at[i], sems.at[i]))
+        arrivals[-1].start()
+    for b in range(blocks):
+        first = b * per_block
+        rows = slice(b * length, (b + 1) * length)
+        for arrival in arrivals[first : first + per_block]:
+            arrival.wait()
+        for h in range(width // HD):
+            cols = slice(h * HD, (h + 1) * HD)
+            keys = keys_ref[first : first + per_block, :, cols].reshape(per_block * PLEN, HD)
+            weights = softmax_turned(keys, q_ref[rows, cols]).astype(jnp.bfloat16)
+            values = dot_nn(weights, gin_ref[rows, cols]).astype(jnp.bfloat16)
+            made_ref[first : first + per_block, :, cols] = values.reshape(per_block, PLEN, HD)
+        for i in range(first, first + per_block):
+            place = out_hbm.at[owner_ref[i - first, b]]
+            sent.append(pltpu.make_async_copy(made_ref.at[i], place, sems.at[len(places) + i]))
+            sent[-1].start()
+    for copy in sent:
+        copy.wait()
+
+
+def value_slots(owner_turned, queries, grad_in, got):
+    slots, length, _ = got.shape
+    count = owner_turned.shape[0] * owner_turned.shape[1]
+    width = queries.shape[1]
+    smem = pl.BlockSpec(memory_space=pltpu.SMEM)
+    vmem = pl.BlockSpec(memory_space=pltpu.VMEM)
+    hbm = pl.BlockSpec(memory_space=pltpu.HBM)
+    pieces = pltpu.VMEM((count, length, width), jnp.bfloat16)
+    return pl.pallas_call(
+        value_slots_kernel,
+        in_specs=[smem, vmem, vmem, hbm],
+        out_specs=hbm,
+        out_shape=pltpu.HBM((slots, length, width), jnp.bfloat16),
+        scratch_shapes=[pieces, pieces, pltpu.SemaphoreType.DMA((2 * count,))],
+        compiler_params=pltpu.CompilerParams(vmem_limit_bytes=12 * MIB),
+        cost_estimate=pl.CostEstimate(
+            flops=4 * queries.size * PLEN * owner_turned.shape[0],
+            bytes_accessed=2 * got.size,
+            transcendentals=queries.size * PLEN * owner_turned.shape[0] // HD,
+        ),
+        name="value_slots",
+    )(owner_turned, queries, grad_in, in_hbm(got))
+
+
+def key_slots_kernel(owner_ref, q_ref, gin_ref, *refs):
+    pieces, (gq_ref, out_hbm, scratch, sems) = refs[:-4], refs[-4:]
     per_block = owner_ref.shape[0]
+    width = q_ref.shape[1]
     each = len(pieces) // per_block
     length = q_ref.shape[0] // each
-    gate = jax.nn.sigmoid(g_ref[...].astype(jnp.float32))
-    grad_in = (gate * c_ref[...].astype(jnp.float32)).astype(jnp.bfloat16)
+    slot = lax.rem(pl.program_id(0), 2)
     units = []
     for b in range(each):
         for h in range(width // HD):
             rows = slice(b * length, (b + 1) * length)
             cols = slice(h * HD, (h + 1) * HD)
+            vcols = slice(width + h * HD, width + (h + 1) * HD)
             own = pieces[b * per_block : (b + 1) * per_block]
             keys = jnp.concatenate([p[0, :, cols] for p in own], axis=0)
-            units.append((b, rows, cols, own, q_ref[rows, cols], grad_in[rows, cols], keys))
-    scores = [dot_nt(u[6], u[4]) * HD ** (-0.5) for u in units]
-    weights = [jnp.exp(x - jnp.max(x, axis=0, keepdims=True)) for x in scores]
-    weights = [x * (1.0 / jnp.sum(x, axis=0, keepdims=True)) for x in weights]
-    return units, weights
-
-
-def value_slots_kernel(owner_ref, q_ref, g_ref, c_ref, *refs):
-    pieces, (out_hbm, scratch, sems) = refs[:-3], refs[-3:]
-    per_block = owner_ref.shape[0]
-    slot = lax.rem(pl.program_id(0), 2)
-    units, weights = block_units(owner_ref, q_ref, g_ref, c_ref, pieces)
+            values = jnp.concatenate([p[0, :, vcols] for p in own], axis=0)
+            q = q_ref[rows, cols]
+            weights = softmax_turned(keys, q)
+            grad_weights = dot_nt(values, gin_ref[rows, cols])
+            kept = weights.astype(jnp.bfloat16).astype(jnp.float32)
+            delta = jnp.sum(kept * grad_weights, axis=0, keepdims=True)
+            half = (weights * (grad_weights - delta)).astype(jnp.bfloat16)
+            units.append((b, rows, cols, q, keys, half))
     wait_slots(owner_ref, scratch, out_hbm, sems)
-    for (b, _, cols, _, _, gin, _), weight in zip(units, weights):
-        grad_values = dot_nn(weight.astype(jnp.bfloat16), gin).astype(jnp.bfloat16)
-        for j in range(per_block):
-            part = slice(j * PLEN, (j + 1) * PLEN)
-            scratch[slot, b * per_block + j, :, cols] = grad_values[part]
-    send_slots(owner_ref, scratch, out_hbm, sems)
-
-
-def key_slots_kernel(owner_ref, q_ref, g_ref, c_ref, *refs):
-    pieces, (gq_ref, out_hbm, scratch, sems) = refs[:-4], refs[-4:]
-    per_block = owner_ref.shape[0]
-    width = q_ref.shape[1]
-    slot = lax.rem(pl.program_id(0), 2)
-    units, weights = block_units(owner_ref, q_ref, g_ref, c_ref, pieces)
-    grad_weights = []
-    for _, _, cols, own, _, gin, _ in units:
-        vcols = slice(width + cols.start, width + cols.stop)
-        values = jnp.concatenate([p[0, :, vcols] for p in own], axis=0)
-        grad_weights.append(dot_nt(values, gin))
-    delta = [
-        jnp.sum(w.astype(jnp.bfloat16).astype(jnp.float32) * g, axis=0, keepdims=True)
-        for w, g in zip(weights, grad_weights)
-    ]
-    halves = [(w * (g - d)).astype(jnp.bfloat16) for w, g, d in zip(weights, grad_weights, delta)]
-    wait_slots(owner_ref, scratch, out_hbm, sems)
-    for (b, rows, cols, _, q, _, keys), half in zip(units, halves):
+    for b, rows, cols, q, keys, half in units:
         gq_ref[rows, cols] = dot_tn(half, keys) * HD ** (-0.5)
         grad_keys = (dot_nn(half, q) * HD ** (-0.5)).astype(jnp.bfloat16)
         for j in range(per_block):
@@ -258,49 +311,43 @@
     send_slots(owner_ref, scratch, out_hbm, sems)
 
 
-def attention(owner_turned, queries, gate_pre, cotangent, got, keys_only):
+def key_slots(owner_turned, queries, grad_in, got):
     rows, width = queries.shape
     per_block, blocks = owner_turned.shape
     slots, length, both = got.shape
     each = 2
     steps = blocks // each
     tokens = pl.BlockSpec((rows // steps, width), lambda i, o: (i, 0))
-    read = width if keys_only else both
 
     def piece(b, j):
-        return pl.BlockSpec((1, length, read), lambda i, o: (o[j, i * each + b], 0, 0))
+        return pl.BlockSpec((1, length, both), lambda i, o: (o[j, i * each + b], 0, 0))
 
     pieces = [piece(b, j) for b in range(each) for j in range(per_block)]
     keys = PLEN * per_block
-    out = pltpu.HBM((slots, length, width), jnp.bfloat16)
-    hbm = pl.BlockSpec(memory_space=pltpu.HBM)
-    return pl.pallas_call(
-        value_slots_kernel if keys_only else key_slots_kernel,
+    return pl.pallas_call(
+        key_slots_kernel,
         grid_spec=pltpu.PrefetchScalarGridSpec(
             num_scalar_prefetch=1,
             grid=(steps,),
-            in_specs=[tokens, tokens, tokens] + pieces,
-            out_specs=[hbm] if keys_only else [tokens, hbm],
+            in_specs=[tokens, tokens] + pieces,
+            out_specs=[tokens, pl.BlockSpec(memory_space=pltpu.HBM)],
             scratch_shapes=[
                 pltpu.VMEM((2, len(pieces), length, width), jnp.bfloat16),
                 pltpu.SemaphoreType.DMA((2, len(pieces))),
             ],
         ),
-        out_shape=[out] if keys_only else [jax.ShapeDtypeStruct((rows, width), jnp.float32), out],
+        out_shape=[
+            jax.ShapeDtypeStruct((rows, width), jnp.float32),
+            pltpu.HBM((slots, length, width), jnp.bfloat16),
+        ],
         compiler_params=params(20),
         cost_estimate=pl.CostEstimate(
-            flops=(4 if keys_only else 8) * rows * width * keys,
+            flops=8 * rows * width * keys,
             bytes_accessed=10 * rows * width + 2 * got.size,
             transcendentals=rows * width * keys // HD,
         ),
-        name="value_slots" if keys_only else "key_slots",
-    )(
-        owner_turned,
-        in_hbm(queries),
-        in_hbm(gate_pre),
-        in_hbm(cotangent),
-        *([in_hbm(got)] * len(pieces)),
-    )
+        name="key_slots",
+    )(owner_turned, queries, grad_in, *([in_hbm(got)] * len(pieces)))
 
 
 def add_asked(asked_ref, back_ref, total):
@@ -559,14 +606,6 @@
     return lax.ppermute(value, "tp", [(i, (i + turn) % 4) for i in range(4)])
 
 
-def halved(value, axis, distance, kind):
-    size = lax.axis_size(axis)
-    half = value.shape[0] // 2
-    pairs = [(i, i ^ distance) for i in range(size)]
-    came = lax.ppermute(value[half:].astype(kind), axis, pairs)
-    return value[:half] + came.astype(jnp.float32)
-
-
 def local(queries, gate_pre, cotangent, store, store_gain, w_key, w_value, owners, slots):
     st_size = lax.axis_size(ST)
     width = queries.shape[1]
@@ -590,12 +629,11 @@
     for turn in (1, 3, 2):
         weights.append(shifted(both, turn))
 
-    (outgoing,) = attention(owner_turned, queries, gate_pre, cotangent, got, True)
+    grad_in = gated(gate_pre, cotangent)
+    outgoing = value_slots(owner_turned, queries, grad_in, got)
     back_values = lax.all_to_all(outgoing, ST, split_axis=0, concat_axis=0, tiled=True)
     late_got, _ = lax.optimization_barrier((got, outgoing))
-    grad_queries, outgoing = attention(
-        owner_turned, queries, gate_pre, cotangent, late_got, False
-    )
+    grad_queries, outgoing = key_slots(owner_turned, queries, grad_in, late_got)
     turned = turned_normed(store, gain)
     outgoing, turned = lax.optimization_barrier((outgoing, turned))
     back_keys = lax.all_to_all(outgoing, ST, split_axis=0, concat_axis=0, tiled=True)
@@ -611,8 +649,13 @@
     near = near_products(parts, weights)
     came = lax.ppermute(other, "st_2", [(0, 1), (1, 0)])
     terms = mine.astype(jnp.float32) + came.astype(jnp.float32)
-    terms = halved(terms, "st_1", 2, jnp.bfloat16)
-    terms = halved(terms, "st_1", 1, jnp.bfloat16)
+    terms = terms.reshape((4, terms.shape[0] // 4) + terms.shape[1:])
+    near_terms = [terms[0]]
+    for distance in (2, 1, 3):
+        pairs = [(i, i ^ distance) for i in range(4)]
+        came = lax.ppermute(terms[distance].astype(jnp.bfloat16), "st_1", pairs)
+        near_terms.append(came.astype(jnp.float32))
+    terms = sum(near_terms)
     back_keys, near = lax.optimization_barrier((back_keys, near))
     spread = [terms[0]]
     for distance in range(1, terms.shape[0]):

time: 351 us -> 349 us (level)
  blocking collectives: 104 us -> 0 us
  waiting for transfers between devices: 137 us -> 226 us
  starting transfers between devices: 54.8 us -> 62.1 us
    all_to_all x1 -> x0, blocking collectives: 104 us -> none  [local(): got = lax.all_to_all(picked, ST, split_axis=0, concat_axis=0, tiled=True)]
    all_to_all x0 -> x1, waiting for transfers between devices: none -> 94 us  [local(): got = lax.all_to_all(picked, ST, split_axis=0, concat_axis=0, tiled=True)]
    all_to_all x0 -> x1, starting transfers between devices: none -> 8.01 us  [local(): got = lax.all_to_all(picked, ST, split_axis=0, concat_axis=0, tiled=True)]
    pallas_call x2 -> x3, Pallas kernels: 13.1 us -> 15.7 us  [the longest x1 7.11 us: key_slots(): pl.pallas_call(key_slots_kernel, grid_spec=pltpu.PrefetchScalarGridSpec(n...]
  transfers between devices with their start and end apart: 22 -> 24, of which waited for: 9 -> 8; matrix products, arithmetic and copies ran while one was open for 0% -> 1% of each run, Pallas kernels for 11% -> 12%
where the time goes in v3:
time: 349 us; the launch traced here: 347 us
  waiting for transfers between devices  226 us (65%)
  starting transfers between devices  62.1 us (18%)
  Pallas kernels  51.7 us (15%)
  other arithmetic  5.55 us (2%)
    all_to_all x1, waiting for transfers between devices, local(): got = lax.all_to_all(picked, ST, split_axis=0, concat_axis=0, tiled=True)  94 us
    ppermute x9, waiting for transfers between devices, shifted(): return lax.ppermute(value, 'tp', [(i, (i + turn) % 4) for i in range(4)])  92.2 us
    all_to_all x2, waiting for transfers between devices, local(): lax.all_to_all(outgoing, ST, split_axis=0, concat_axis=0, tiled=True)  36.5 us
    ppermute x7, starting transfers between devices, local(): spread.append(lax.ppermute(terms[distance], 'st_0', pairs))  14.4 us
    ppermute x9, starting transfers between devices, shifted(): return lax.ppermute(value, 'tp', [(i, (i + turn) % 4) for i in range(4)])  12.3 us
    all_to_all x1, starting transfers between devices, local(): lax.all_to_all(requests, ST, split_axis=0, concat_axis=0, tiled=True)  12.1 us
    all_to_all x2, starting transfers between devices, local(): lax.all_to_all(outgoing, ST, split_axis=0, concat_axis=0, tiled=True)  10.8 us
    pallas_call x1, Pallas kernels, key_value_tables(): pl.pallas_call(tables_kernel, grid=(rows // step,), in_specs=[pl.BlockSpe...  8.32 us
  transfers between devices with their start and end apart: 24, of which 8 were waited for; matrix products, arithmetic and copies ran while one was open for 1% of the time, Pallas kernels for 12%

profile of v3, /device:TPU:2, one launch (start us, length us, event | category | flops | bytes accessed | tf_op | source)
XLA Modules:
  0.0 346.8 jit_solution(14481019488629626022)
XLA Ops:
  2.0 12.1 %all-to-all-start = ((s32[64,4,8]{2,1,0:T(4,128)}), s32[64,4,8]{2,1,0:T(4,128)S(1)}, u32[]{:S(2)}, u32[]{:S(2)}) async-start(s32[64,4,8]{2,1,0:T(4,128)} %fusion.2), calls=%async_computation | async-start | bytes 262144 | tf_op jit(solution)/shard_map/all_to_all | solution.py:620
  14.1 8.3 %tables.1 = (bf16[1280,512]{1,0:T(8,128)(2,1)S(1)}, bf16[2048,512]{1,0:T(8,128)(2,1)}) custom-call(bf16[1280,2048]{1,0:T(8,128)(2,1)} %refs_4_.1, f32[1,2048]{1,0:T(1,128)} %bitcast.37, bf16[2048,256]{1,0:T(8,128)(2,1)} %wk_hbm.1, bf16[2048,256]{1,0:T(8,128)(2,1)} %wv_hbm.1), custom_call_target="tpu_custom_call" | custom-call | flops 2684354560 | bytes 5242880 | tf_op jit(solution)/shard_map/tables/pallas_call | solution.py:81
  22.5 2.7 all-to-all-done
  26.4 3.1 picked.1
  29.5 8.0 %all-to-all-start.1 = ((bf16[64,64,512]{2,1,0:T(8,128)(2,1)}), bf16[64,64,512]{2,1,0:T(8,128)(2,1)}, u32[]{:S(2)}, u32[]{:S(2)}) async-start(bf16[64,64,512]{2,1,0:T(8,128)(2,1)} %picked.1), calls=%async_computation.1 | async-start | bytes 8388608 | tf_op jit(solution)/shard_map/all_to_all | solution.py:625
  37.5 2.2 gated.1.gin_ref
  39.8 94.0 %all-to-all-done.1.got_hbm.refs_0_.refs_1_.refs_2_.refs_3_.refs_4_.refs_5_.refs_6_.refs_7_ = bf16[64,64,512]{2,1,0:T(8,128)(2,1)} async-done(((bf16[64,64,512]{2,1,0:T(8,128)(2,1)}), bf16[64,64,512]{2,1,0:T(8,128)(2,1)}, u32[]{:S(2)}, u32[]{:S(2)}) %all-to-all-start.1) | async-done | bytes 4194336 | tf_op jit(solution)/shard_map/all_to_all | solution.py:625
  133.8 6.4 %value_slots.1 = bf16[64,64,256]{2,1,0:T(8,128)(2,1)} custom-call(s32[4,8]{1,0:T(4,128)S(1)} %bitcast.41, bf16[1024,256]{1,0:T(8,128)(2,1)S(1)} %copy-done, bf16[1024,256]{1,0:T(8,128)(2,1)S(1)} %gated.1.gin_ref, bf16[64,64,512]{2,1,0:T(8,128)(2,1)} %all-to-all-done.1.got_hbm.refs_0_.refs_1_.refs_2_.refs_3_.refs_4_.refs_5_.refs_6_.refs_7_), custom_call_target="tpu_custom_call" | custom-call | flops 268435456 | bytes 4194304 | tf_op jit(solution)/shard_map/value_slots/pallas_call | solution.py:265
  140.2 5.2 %all-to-all-start.3 = ((bf16[64,64,256]{2,1,0:T(8,128)(2,1)}), bf16[64,64,256]{2,1,0:T(8,128)(2,1)S(1)}, u32[]{:S(2)}, u32[]{:S(2)}) async-start(bf16[64,64,256]{2,1,0:T(8,128)(2,1)} %value_slots.1), calls=%async_computation.3 | async-start | bytes 4194304 | tf_op jit(solution)/shard_map/all_to_all | solution.py:634
  145.4 7.8 %turned_normed.1.turned_hbm = bf16[2048,1280]{1,0:T(8,128)(2,1)} custom-call(bf16[1280,2048]{1,0:T(8,128)(2,1)} %refs_4_.1, f32[1,2048]{1,0:T(1,128)} %bitcast.38), custom_call_target="tpu_custom_call" | custom-call | flops 41943040 | bytes 10485760 | tf_op jit(solution)/shard_map/turned_normed/pallas_call | solution.py:119
  153.1 7.1 %key_slots.1 = (f32[1024,256]{1,0:T(8,128)}, bf16[64,64,256]{2,1,0:T(8,128)(2,1)}) custom-call(s32[4,8]{1,0:T(4,128)S(1)} %bitcast.42, bf16[1024,256]{1,0:T(8,128)(2,1)S(1)} %copy-done, bf16[1024,256]{1,0:T(8,128)(2,1)S(1)} %gated.1.gin_ref, bf16[64,64,512]{2,1,0:T(8,128)(2,1)} %all-to-all-done.1.got_hbm.refs_0_.refs_1_.refs_2_.refs_3_.refs_4_.refs_5_.refs_6_.refs_7_, ...), custom_call_target="tpu_custom_call" | custom-call | flops 536870912 | bytes 6815744 | tf_op jit(solution)/shard_map/key_slots/pallas_call | solution.py:327
  160.3 36.5 %all-to-all-done.3.back_ref = bf16[64,64,256]{2,1,0:T(8,128)(2,1)S(1)} async-done(((bf16[64,64,256]{2,1,0:T(8,128)(2,1)}), bf16[64,64,256]{2,1,0:T(8,128)(2,1)S(1)}, u32[]{:S(2)}, u32[]{:S(2)}) %all-to-all-start.3) | async-done | bytes 2097184 | tf_op jit(solution)/shard_map/all_to_all | solution.py:634
  196.7 5.6 %all-to-all-start.2 = ((bf16[64,64,256]{2,1,0:T(8,128)(2,1)}), bf16[64,64,256]{2,1,0:T(8,128)(2,1)}, u32[]{:S(2)}, u32[]{:S(2)}) async-start(bf16[64,64,256]{2,1,0:T(8,128)(2,1)} %get-tuple-element.37), calls=%async_computation.2 | async-start | bytes 4194304 | tf_op jit(solution)/shard_map/all_to_all | solution.py:639
  206.6 46.1 %collective-permute-done.2.refs_7_.refs_3_ = bf16[2048,512]{1,0:T(8,128)(2,1)} collective-permute-done((bf16[2048,512]{1,0:T(8,128)(2,1)}, bf16[2048,512]{1,0:T(8,128)(2,1)}, u32[]{:S(2)}, u32[]{:S(2)}) %collective-permute-start.2) | collective-permute-done | bytes 2097184 | tf_op jit(solution)/shard_map/ppermute | solution.py:606
  252.8 43.9 %collective-permute-done.1.refs_6_.refs_2_ = bf16[2048,512]{1,0:T(8,128)(2,1)} collective-permute-done((bf16[2048,512]{1,0:T(8,128)(2,1)}, bf16[2048,512]{1,0:T(8,128)(2,1)}, u32[]{:S(2)}, u32[]{:S(2)}) %collective-permute-start.1) | collective-permute-done | bytes 2097184 | tf_op jit(solution)/shard_map/ppermute | solution.py:606
  296.8 4.7 %value_sums.1 = (bf16[320,256]{1,0:T(8,128)(2,1)S(1)}, bf16[320,256]{1,0:T(8,128)(2,1)S(1)}, bf16[320,256]{1,0:T(8,128)(2,1)S(1)}, bf16[320,256]{1,0:T(8,128)(2,...) custom-call(s32[64]{0:T(128)S(1)} %reduce_max.9.asked_ref, s32[2]{0:T(128)S(1)} %pad_add_fusion.place_ref, ...), custom_call_target="tpu_custom_call" | custom-call | flops 1342177280 | bytes 5242880 | tf_op jit(solution)/shard_map/value_sums/pallas_call | solution.py:410
  306.9 3.2 collective-permute-start.10
  313.4 3.4 near_products.1.near_ref
  316.9 2.4 key_sums.1
  326.0 2.9 collective-permute-start.19
  328.8 3.2 own_product.1
  333.2 3.9 %collective-permute-start.17 = (f32[32,256]{1,0:T(8,128)S(1)}, f32[32,256]{1,0:T(8,128)S(1)}, u32[]{:S(2)}, u32[]{:S(2)}) collective-permute-start(f32[32,256]{1,0:T(8,128)S(1)} %get-tuple-element.71), channel_id=1, source_target_pairs={{0,160},{32,128},{64,224},{96,192},{128,32},{160,0},{192,96},{224,... | collective-permute-start | bytes 98312 | tf_op jit(solution)/shard_map/ppermute | solution.py:663
  339.0 2.4 collective-permute-start.15
  341.8 3.2 store_gradient.1
  (49 shorter events, 27.6 us)
Async XLA Ops:
  2.0 23.1 %all-to-all-start = ((s32[64,4,8]{2,1,0:T(4,128)}), s32[64,4,8]{2,1,0:T(4,128)S(1)}, u32[]{:S(2)}, u32[]{:S(2)}) async-start(s32[64,4,8]{2,1,0:T(4,128)} %fusion.2), calls=%async_computation | async-start | bytes 262144 | tf_op jit(solution)/shard_map/all_to_all | solution.py:620
  29.5 104.3 %all-to-all-start.1 = ((bf16[64,64,512]{2,1,0:T(8,128)(2,1)}), bf16[64,64,512]{2,1,0:T(8,128)(2,1)}, u32[]{:S(2)}, u32[]{:S(2)}) async-start(bf16[64,64,512]{2,1,0:T(8,128)(2,1)} %picked.1), calls=%async_computation.1 | async-start | bytes 8388608 | tf_op jit(solution)/shard_map/all_to_all | solution.py:625
  140.2 56.6 %all-to-all-start.3 = ((bf16[64,64,256]{2,1,0:T(8,128)(2,1)}), bf16[64,64,256]{2,1,0:T(8,128)(2,1)S(1)}, u32[]{:S(2)}, u32[]{:S(2)}) async-start(bf16[64,64,256]{2,1,0:T(8,128)(2,1)} %value_slots.1), calls=%async_computation.3 | async-start | bytes 4194304 | tf_op jit(solution)/shard_map/all_to_all | solution.py:634
  196.7 120.1 %all-to-all-start.2 = ((bf16[64,64,256]{2,1,0:T(8,128)(2,1)}), bf16[64,64,256]{2,1,0:T(8,128)(2,1)}, u32[]{:S(2)}, u32[]{:S(2)}) async-start(bf16[64,64,256]{2,1,0:T(8,128)(2,1)} %get-tuple-element.37), calls=%async_computation.2 | async-start | bytes 4194304 | tf_op jit(solution)/shard_map/all_to_all | solution.py:639
  202.3 50.5 %collective-permute-start.2 = (bf16[2048,512]{1,0:T(8,128)(2,1)}, bf16[2048,512]{1,0:T(8,128)(2,1)}, u32[]{:S(2)}, u32[]{:S(2)}) collective-permute-start(bf16[2048,512]{1,0:T(8,128)(2,1)} %get-tuple-element.40.refs_4_.refs_0_), channel_id=1, source_target_pairs={{0,2},{1,3},{2,0},{3,1},{4,6},{5,7},{6,4},{7,5},{8,10},{9,11},{10,... | collective-permute-start | bytes 6291464 | tf_op jit(solution)/shard_map/ppermute | solution.py:606
  204.5 92.2 %collective-permute-start.1 = (bf16[2048,512]{1,0:T(8,128)(2,1)}, bf16[2048,512]{1,0:T(8,128)(2,1)}, u32[]{:S(2)}, u32[]{:S(2)}) collective-permute-start(bf16[2048,512]{1,0:T(8,128)(2,1)} %get-tuple-element.40.refs_4_.refs_0_), channel_id=1, source_target_pairs={{0,3},{1,0},{2,1},{3,2},{4,7},{5,4},{6,5},{7,6},{8,11},{9,8},{10,9... | collective-permute-start | bytes 6291464 | tf_op jit(solution)/shard_map/ppermute | solution.py:606
  206.0 90.8 %collective-permute-start = (bf16[2048,512]{1,0:T(8,128)(2,1)}, bf16[2048,512]{1,0:T(8,128)(2,1)}, u32[]{:S(2)}, u32[]{:S(2)}) collective-permute-start(bf16[2048,512]{1,0:T(8,128)(2,1)} %get-tuple-element.40.refs_4_.refs_0_), channel_id=1, source_target_pairs={{0,1},{1,2},{2,3},{3,0},{4,5},{5,6},{6,7},{7,4},{8,9},{9,10},{10,1... | collective-permute-start | bytes 6291464 | tf_op jit(solution)/shard_map/ppermute | solution.py:606
  301.4 4.3 %collective-permute-start.9 = (bf16[32,32,256]{2,1,0:T(8,128)(2,1)S(1)}, bf16[32,32,256]{2,1,0:T(8,128)(2,1)S(1)}, u32[]{:S(2)}, u32[]{:S(2)}) collective-permute-start(bf16[32,32,256]{2,1,0:T(8,128)(2,1)S(1)} %get-tuple-element.62), channel_id=1, source_target_pairs={{0,4},{4,0},{1,5},{5,1},{2,6},{6,2},{3,7},{7,3},{8,12},{12,8},{9,1... | collective-permute-start | bytes 1572872 | tf_op jit(solution)/shard_map/ppermute | solution.py:650
  301.5 9.8 %collective-permute-start.3 = (bf16[320,256]{1,0:T(8,128)(2,1)S(1)}, bf16[320,256]{1,0:T(8,128)(2,1)S(1)}, u32[]{:S(2)}, u32[]{:S(2)}) collective-permute-start(bf16[320,256]{1,0:T(8,128)(2,1)S(1)} %get-tuple-element.44), channel_id=1, source_target_pairs={{0,1},{1,2},{2,3},{3,0},{4,5},{5,6},{6,7},{7,4},{8,9},{9,10},{10,1... | collective-permute-start | bytes 491528 | tf_op jit(solution)/shard_map/ppermute | solution.py:606
  303.0 8.3 %collective-permute-start.4 = (bf16[320,256]{1,0:T(8,128)(2,1)S(1)}, bf16[320,256]{1,0:T(8,128)(2,1)S(1)}, u32[]{:S(2)}, u32[]{:S(2)}) collective-permute-start(bf16[320,256]{1,0:T(8,128)(2,1)S(1)} %get-tuple-element.45), channel_id=1, source_target_pairs={{0,3},{1,0},{2,1},{3,2},{4,7},{5,4},{6,5},{7,6},{8,11},{9,8},{10,9... | collective-permute-start | bytes 491528 | tf_op jit(solution)/shard_map/ppermute | solution.py:606
  303.6 9.8 %collective-permute-start.5 = (bf16[320,256]{1,0:T(8,128)(2,1)S(1)}, bf16[320,256]{1,0:T(8,128)(2,1)S(1)}, u32[]{:S(2)}, u32[]{:S(2)}) collective-permute-start(bf16[320,256]{1,0:T(8,128)(2,1)S(1)} %get-tuple-element.46), channel_id=1, source_target_pairs={{0,2},{1,3},{2,0},{3,1},{4,6},{5,7},{6,4},{7,5},{8,10},{9,11},{10,... | collective-permute-start | bytes 491528 | tf_op jit(solution)/shard_map/ppermute | solution.py:606
  306.9 14.4 %collective-permute-start.10 = (bf16[8,32,256]{2,1,0:T(8,128)(2,1)S(1)}, bf16[8,32,256]{2,1,0:T(8,128)(2,1)S(1)}, u32[]{:S(2)}, u32[]{:S(2)}) collective-permute-start(bf16[8,32,256]{2,1,0:T(8,128)(2,1)S(1)} %get-tuple-element.65), channel_id=1, source_target_pairs={{0,16},{8,24},{16,0},{24,8},{1,17},{9,25},{17,1},{25,9},{2,18},{10... | collective-permute-start | bytes 393224 | tf_op jit(solution)/shard_map/ppermute | solution.py:656
  310.2 13.0 %collective-permute-start.12 = (bf16[8,32,256]{2,1,0:T(8,128)(2,1)S(1)}, bf16[8,32,256]{2,1,0:T(8,128)(2,1)S(1)}, u32[]{:S(2)}, u32[]{:S(2)}) collective-permute-start(bf16[8,32,256]{2,1,0:T(8,128)(2,1)S(1)} %get-tuple-element.66), channel_id=1, source_target_pairs={{0,24},{8,16},{16,8},{24,0},{1,25},{9,17},{17,9},{25,1},{2,26},{10... | collective-permute-start | bytes 393224 | tf_op jit(solution)/shard_map/ppermute | solution.py:656
  311.3 11.8 %collective-permute-start.11 = (bf16[8,32,256]{2,1,0:T(8,128)(2,1)S(1)}, bf16[8,32,256]{2,1,0:T(8,128)(2,1)S(1)}, u32[]{:S(2)}, u32[]{:S(2)}) collective-permute-start(bf16[8,32,256]{2,1,0:T(8,128)(2,1)S(1)} %get-tuple-element.67), channel_id=1, source_target_pairs={{0,8},{8,0},{16,24},{24,16},{1,9},{9,1},{17,25},{25,17},{2,10},{10... | collective-permute-start | bytes 393224 | tf_op jit(solution)/shard_map/ppermute | solution.py:656
  319.2 12.8 %collective-permute-start.6 = (bf16[320,256]{1,0:T(8,128)(2,1)S(1)}, bf16[320,256]{1,0:T(8,128)(2,1)S(1)}, u32[]{:S(2)}, u32[]{:S(2)}) collective-permute-start(bf16[320,256]{1,0:T(8,128)(2,1)S(1)} %get-tuple-element.55), channel_id=1, source_target_pairs={{0,1},{1,2},{2,3},{3,0},{4,5},{5,6},{6,7},{7,4},{8,9},{9,10},{10,1... | collective-permute-start | bytes 491528 | tf_op jit(solution)/shard_map/ppermute | solution.py:606
  319.3 13.9 %collective-permute-start.7 = (bf16[320,256]{1,0:T(8,128)(2,1)S(1)}, bf16[320,256]{1,0:T(8,128)(2,1)S(1)}, u32[]{:S(2)}, u32[]{:S(2)}) collective-permute-start(bf16[320,256]{1,0:T(8,128)(2,1)S(1)} %get-tuple-element.56), channel_id=1, source_target_pairs={{0,3},{1,0},{2,1},{3,2},{4,7},{5,4},{6,5},{7,6},{8,11},{9,8},{10,9... | collective-permute-start | bytes 491528 | tf_op jit(solution)/shard_map/ppermute | solution.py:606
  321.3 15.8 %collective-permute-start.8 = (bf16[320,256]{1,0:T(8,128)(2,1)S(1)}, bf16[320,256]{1,0:T(8,128)(2,1)S(1)}, u32[]{:S(2)}, u32[]{:S(2)}) collective-permute-start(bf16[320,256]{1,0:T(8,128)(2,1)S(1)} %get-tuple-element.57), channel_id=1, source_target_pairs={{0,2},{1,3},{2,0},{3,1},{4,6},{5,7},{6,4},{7,5},{8,10},{9,11},{10,... | collective-permute-start | bytes 491528 | tf_op jit(solution)/shard_map/ppermute | solution.py:606
  324.2 14.7 %collective-permute-start.13 = (f32[32,256]{1,0:T(8,128)S(1)}, f32[32,256]{1,0:T(8,128)S(1)}, u32[]{:S(2)}, u32[]{:S(2)}) collective-permute-start(f32[32,256]{1,0:T(8,128)S(1)} %get-tuple-element.68), channel_id=1, source_target_pairs={{0,32},{32,0},{64,96},{96,64},{128,160},{160,128},{192,224},{224,1... | collective-permute-start | bytes 98312 | tf_op jit(solution)/shard_map/ppermute | solution.py:663
  326.0 15.4 %collective-permute-start.19 = (f32[32,256]{1,0:T(8,128)S(1)}, f32[32,256]{1,0:T(8,128)S(1)}, u32[]{:S(2)}, u32[]{:S(2)}) collective-permute-start(f32[32,256]{1,0:T(8,128)S(1)} %get-tuple-element.69), channel_id=1, source_target_pairs={{0,224},{32,192},{64,160},{96,128},{128,96},{160,64},{192,32},{224... | collective-permute-start | bytes 98312 | tf_op jit(solution)/shard_map/ppermute | solution.py:663
  332.0 13.0 %collective-permute-start.18 = (f32[32,256]{1,0:T(8,128)S(1)}, f32[32,256]{1,0:T(8,128)S(1)}, u32[]{:S(2)}, u32[]{:S(2)}) collective-permute-start(f32[32,256]{1,0:T(8,128)S(1)} %get-tuple-element.70), channel_id=1, source_target_pairs={{0,192},{32,224},{64,128},{96,160},{128,64},{160,96},{192,0},{224,... | collective-permute-start | bytes 98312 | tf_op jit(solution)/shard_map/ppermute | solution.py:663
  333.2 11.9 %collective-permute-start.17 = (f32[32,256]{1,0:T(8,128)S(1)}, f32[32,256]{1,0:T(8,128)S(1)}, u32[]{:S(2)}, u32[]{:S(2)}) collective-permute-start(f32[32,256]{1,0:T(8,128)S(1)} %get-tuple-element.71), channel_id=1, source_target_pairs={{0,160},{32,128},{64,224},{96,192},{128,32},{160,0},{192,96},{224,... | collective-permute-start | bytes 98312 | tf_op jit(solution)/shard_map/ppermute | solution.py:663
  337.1 8.0 %collective-permute-start.16 = (f32[32,256]{1,0:T(8,128)S(1)}, f32[32,256]{1,0:T(8,128)S(1)}, u32[]{:S(2)}, u32[]{:S(2)}) collective-permute-start(f32[32,256]{1,0:T(8,128)S(1)} %get-tuple-element.72), channel_id=1, source_target_pairs={{0,128},{32,160},{64,192},{96,224},{128,0},{160,32},{192,64},{224,... | collective-permute-start | bytes 98312 | tf_op jit(solution)/shard_map/ppermute | solution.py:663
  339.0 6.2 %collective-permute-start.15 = (f32[32,256]{1,0:T(8,128)S(1)}, f32[32,256]{1,0:T(8,128)S(1)}, u32[]{:S(2)}, u32[]{:S(2)}) collective-permute-start(f32[32,256]{1,0:T(8,128)S(1)} %get-tuple-element.73), channel_id=1, source_target_pairs={{0,96},{32,64},{64,32},{96,0},{128,224},{160,192},{192,160},{224,1... | collective-permute-start | bytes 98312 | tf_op jit(solution)/shard_map/ppermute | solution.py:663
  341.3 4.8 %collective-permute-start.14 = (f32[32,256]{1,0:T(8,128)S(1)}, f32[32,256]{1,0:T(8,128)S(1)}, u32[]{:S(2)}, u32[]{:S(2)}) collective-permute-start(f32[32,256]{1,0:T(8,128)S(1)} %get-tuple-element.74), channel_id=1, source_target_pairs={{0,64},{32,96},{64,0},{96,32},{128,192},{160,224},{192,128},{224,1... | collective-permute-start | bytes 98312 | tf_op jit(solution)/shard_map/ppermute | solution.py:663
  (3 other events, 221.6 us)
